TPU v7x, 256 devices: a 4x2x16 block of a 4x16x16 slice. The times are simulated.
256 devices in a mesh: grp: 2 (over y), sp: 16 (over z), tp: 8 (over x, core).
Axes of the slice: x: 4, y: 2, z: 16, core: 2. Of those that a mesh axis runs over, the one named last changes fastest.
The devices are a block of a 4x16x16 slice.
Arguments:
- layer_feed: bfloat16 [4, 8192, 4096], P('grp', 'sp'), parts along dimension 0, may hold values from -13 to 13
- address_mapping: bfloat16 [4096, 2048], P(None, 'tp'), may hold values from -0.09375 to 0.09375
- content_mapping: bfloat16 [4096, 2048], P(None, 'tp'), may hold values from -0.09375 to 0.09375
- beta_mapping_matrix: bfloat16 [4096, 32], replicated, may hold values from -0.032958984 to 0.029541016
- forgetting_mapping: bfloat16 [4096, 32], replicated, may hold values from -0.09375 to 0.09375
- logged_fading_speed: float32 [32], P('tp'), may hold values from -12 to -2.8
- extra_forgetting: bfloat16 [4, 8192, 32], P('grp', 'sp', 'tp'), parts along dimension 0, may hold values from -1.4 to 0
- opening_probe: bfloat16 [4, 2048], P('grp', 'tp'), parts along dimension 0, may hold values from -6 to 6
Outputs:
- context_memory_tensor: bfloat16 [4, 32, 64, 64], P('grp', 'tp', 'sp'), parts along dimension 0
- opening_normed_output: bfloat16 [4, 2048], P('grp', 'tp'), parts along dimension 0
There are 2 independent parts, one for each index of `grp`. A program takes and returns all parts, laid end to end along the dimension named above; an argument that names none is the same for every part. Nothing has to cross between parts.
All inputs are finite; a program needn't handle non-finite values.
Results may differ from a plain program's by a relative error of at most 0.014.
Values sent between devices are 32-bit elements; how exact they have to be, the bound alone decides.
No kernel may reach another device: no remote copies, remote signals or barrier semaphores. Data moves between devices by JAX's collectives and lax.ppermute only.
A program may use at most 64 MiB of HBM per device.

v0:
```python
import math

import jax
import jax.numpy as jnp
from jax import lax
from jax.sharding import PartitionSpec as P

HEAD = 64


finest = lax.Precision.HIGHEST


def prefix(part, axis, combine, identity):
    count = lax.axis_size(axis)
    place = lax.axis_index(axis)
    ahead = count - 1 - place
    gathered = lax.all_gather(part, axis)
    state = jnp.zeros_like(part) + jnp.asarray(identity, part.dtype)

    def one(hop, state):
        source = count - 1 - hop
        return combine(state, lax.dynamic_index_in_dim(gathered, source, 0, False))

    return lax.fori_loop(0, ahead, one, state)


def in_blocks(x, dim, size):
    shape = x.shape
    pieces = x.reshape(*shape[:dim], size, shape[dim] // size, *shape[dim + 1 :])
    return jnp.moveaxis(pieces, dim, 0)


def sent_and_summed(x, axis, dim):
    pieces = in_blocks(x, dim, lax.axis_size(axis))
    arrived = lax.all_to_all(pieces, axis, split_axis=0, concat_axis=0, tiled=True)
    return arrived.sum(axis=0)


def sent_to_all(x, axis):
    size = lax.axis_size(axis)
    return lax.all_to_all(jnp.broadcast_to(x[None], (size, *x.shape)), axis, 0, 0, tiled=True)


def taken_together(x, axis):
    return sent_to_all(x, axis).sum(axis=0)


def head_columns(weight, heads):
    first = lax.axis_index("tp") * heads
    return lax.dynamic_slice_in_dim(weight, first, heads, 1)


def compute_states(
    address_embeddings,
    content_embeddings,
    beta_raw_scores,
    forgetting_raw_scores,
    extra_forgetting,
    logged_fading_speed,
):
    seqs, length, width = address_embeddings.shape
    heads = width // HEAD
    keys = jax.nn.silu(address_embeddings.astype(jnp.float32)).reshape(seqs, length, heads, HEAD)
    keys = keys * lax.rsqrt(jnp.sum(keys * keys, axis=-1, keepdims=True) + 1e-06)
    values = jax.nn.silu(content_embeddings.astype(jnp.float32)).reshape(seqs, length, heads, HEAD)
    betas = jax.nn.sigmoid(beta_raw_scores.astype(jnp.float32))
    decay_factors = -jnp.exp(logged_fading_speed) * jax.nn.softplus(
        forgetting_raw_scores.astype(jnp.float32)
    ) + extra_forgetting.astype(jnp.float32)
    groups = seqs * heads
    keys = keys.transpose(0, 2, 1, 3).reshape(groups, length, HEAD)
    values = values.transpose(0, 2, 1, 3).reshape(groups, length, HEAD)
    betas = betas.transpose(0, 2, 1).reshape(groups, length)
    decay_factors = decay_factors.transpose(0, 2, 1).reshape(groups, length)
    return (keys, values, betas, decay_factors)


def block_parts(keys, values, betas, decay_factors):
    groups, length, width = keys.shape
    size = math.gcd(length, 64)
    count = length // size
    keys = keys.reshape(groups, count, size, width)
    values = values.reshape(groups, count, size, width)
    betas = betas.reshape(groups, count, size)
    cumul = jnp.cumsum(decay_factors.reshape(groups, count, size), axis=-1)
    rows_idx = lax.broadcasted_iota(jnp.int32, (size, size), 0)
    cols_idx = lax.broadcasted_iota(jnp.int32, (size, size), 1)
    below = rows_idx > cols_idx
    spread = jnp.where(below, cumul[..., :, None] - cumul[..., None, :], 0.0)
    weights = jnp.where(below, jnp.exp(spread), 0.0)
    gram = jnp.einsum("gnid,gnjd->gnij", keys, keys, precision=finest)
    lower = jnp.eye(size, dtype=jnp.float32) + betas[..., :, None] * gram * weights
    right = jnp.concatenate(
        [values * betas[..., None], keys * (betas * jnp.exp(cumul))[..., None]], axis=-1
    )
    solved = jax.scipy.linalg.solve_triangular(lower, right, lower=True)
    update = solved[..., :width]
    mixing = solved[..., width:]
    carried = keys * jnp.exp(cumul[..., -1:] - cumul)[..., None]
    closing = jnp.exp(cumul[..., -1])
    return (update, mixing, carried, closing)


def run_blocks(start, parts, padding):

    def advance(state, piece):
        update, mixing, carried, closing = piece
        update = jnp.concatenate(
            [jnp.zeros(update.shape[:-1] + (padding,), jnp.float32), update], axis=-1
        )
        fresh = update - jnp.einsum("gck,gkw->gcw", mixing, state, precision=finest)
        state = closing[:, None, None] * state + jnp.einsum(
            "gck,gcw->gkw", carried, fresh, precision=finest
        )
        return (state, None)

    moved = tuple((jnp.moveaxis(member, 1, 0) for member in parts))
    final, _ = lax.scan(advance, start, moved)
    return final


def matmul(left, right):
    return jnp.einsum("shij,shjk->shik", left, right, precision=finest)


def body(
    layer_feed,
    address_mapping,
    content_mapping,
    beta_mapping_matrix,
    forgetting_mapping,
    logged_fading_speed,
    extra_forgetting,
    opening_probe,
):
    heads = address_mapping.shape[1] // HEAD
    seqs_all = layer_feed.shape[0]
    address_embeddings = jnp.dot(
        layer_feed, address_mapping, preferred_element_type=jnp.float32
    ).astype(jnp.bfloat16)
    content_embeddings = jnp.dot(
        layer_feed, content_mapping, preferred_element_type=jnp.float32
    ).astype(jnp.bfloat16)
    beta_raw_scores = jnp.dot(
        layer_feed, head_columns(beta_mapping_matrix, heads), preferred_element_type=jnp.float32
    ).astype(jnp.bfloat16)
    forgetting_raw_scores = jnp.dot(
        layer_feed, head_columns(forgetting_mapping, heads), preferred_element_type=jnp.float32
    ).astype(jnp.bfloat16)
    keys, values, betas, decay_factors = compute_states(
        address_embeddings,
        content_embeddings,
        beta_raw_scores,
        forgetting_raw_scores,
        extra_forgetting,
        logged_fading_speed,
    )
    parts = block_parts(keys, values, betas, decay_factors)
    opening = jnp.concatenate(
        [jnp.eye(HEAD, dtype=jnp.float32), jnp.zeros((HEAD, HEAD), jnp.float32)], axis=1
    )
    start = jnp.broadcast_to(opening, (seqs_all * heads, HEAD, 2 * HEAD))
    joined = run_blocks(start, parts, HEAD).reshape(seqs_all, heads, HEAD, 2 * HEAD)
    transfer = joined[..., :HEAD]
    offset = joined[..., HEAD:]
    identity = jnp.broadcast_to(jnp.eye(HEAD, dtype=jnp.float32), transfer.shape)
    rows = HEAD // lax.axis_size("sp")
    first_row = lax.axis_index("sp") * rows
    suffix = prefix(transfer, "sp", matmul, identity)
    terms = matmul(suffix, offset)
    final = sent_and_summed(terms, "sp", 2)
    context_memory_tensor = final.astype(jnp.bfloat16)
    query_per_head = opening_probe.reshape(seqs_all, heads, HEAD)
    query_rows = lax.dynamic_slice_in_dim(query_per_head, first_row, rows, 2).astype(jnp.float32)
    partial_read = jnp.einsum("shk,shkv->shv", query_rows, final, precision=finest)
    state_readout = taken_together(partial_read, "sp")
    state_readout = state_readout * lax.rsqrt(
        jnp.mean(state_readout * state_readout, axis=-1, keepdims=True) + 1e-06
    )
    opening_normed_output = state_readout.reshape(seqs_all, heads * HEAD).astype(jnp.bfloat16)
    return (context_memory_tensor, opening_normed_output)


def solution(mesh):
    in_specs = (
        P("grp", "sp", None),
        P(None, "tp"),
        P(None, "tp"),
        P(),
        P(),
        P("tp"),
        P("grp", "sp", "tp"),
        P("grp", "tp"),
    )
    out_specs = (P("grp", "tp", "sp", None), P("grp", "tp"))
    return jax.shard_map(body, mesh=mesh, in_specs=in_specs, out_specs=out_specs, check_vma=False)
```

profile of v0, /device:TPU:46, one launch (start us, length us, event | category | flops | bytes accessed | tf_op | source)
XLA Modules:
  0.0 566.3 jit_solution(1860633266186598040)
XLA Ops:
  8.1 5.7 %fusion.52 = f32[2,4,512]{2,1,0:T(4,128)S(1)} fusion(bf16[2,512,4]{1,2,0:T(4,128)(2,1)} %param.18, bf16[2,512,4096]{2,1,0:T(8,128)(2,1)} %param.12, bf16[4096,32]{0,1:T(8,128)(2,1)} %param.16, s32[]{:T(128)S(6)} %select_n.25, f32[4]{0:T(128)S(1)} %exponential_negate_fusion), kind=kOutput, calls=%fused_computation.71 | convolution fusion | flops 33599488 | bytes 8445972 | tf_op jit(solution)/shard_map/dot_general | solution.py:148
  13.9 1.9 reduce_window_sum.11
  15.9 5.7 %fusion.30 = f32[2,4,512]{2,1,0:T(4,128)S(1)} fusion(bf16[2,512,4096]{2,1,0:T(8,128)(2,1)} %param.12, bf16[4096,32]{0,1:T(8,128)(2,1)} %param.15, s32[]{:T(128)S(6)} %select_n.25), kind=kOutput, calls=%fused_computation.40 | convolution fusion | flops 33574912 | bytes 8437764 | tf_op jit(solution)/shard_map/dot_general | solution.py:145
  21.8 6.0 %multiply_reduce_fusion = (f32[2,512,4]{1,2,0:T(4,128)S(1)}, f32[2,512,256]{1,2,0:T(8,128)S(1)}) fusion(bf16[2,512,4096]{2,1,0:T(8,128)(2,1)} %param.12, bf16[4096,256]{1,0:T(8,128)(2,1)S(1)} %copy-done), kind=kOutput, calls=%fused_computation.53 | convolution fusion | flops 2149576704 | bytes 11550720 | tf_op jit(solution)/shard_map/dot_general | solution.py:139
  27.8 2.0 copy.67
  29.8 2.2 broadcast_multiply_fusion.2
  33.3 4.8 select_bitcast_fusion
  38.1 316.0 %custom-call.4 = f32[8,8,1,64,64]{3,4,2,1,0:T(8,128)} custom-call(f32[8,8,1,64,64]{4,3,2,1,0:T(8,128)} %select_bitcast_fusion), custom_call_target="InvertDiagBlocksLowerTriangular" | custom-call | tf_op jit(solution)/shard_map/jit(_solve_triangular)/vmap(vmap())/triangular_solve | solution.py:97
  354.1 6.5 %convert_multiply_fusion = f32[2,512,256]{1,2,0:T(8,128)S(1)} fusion(bf16[2,512,4096]{2,1,0:T(8,128)(2,1)} %param.12, bf16[4096,256]{1,0:T(8,128)(2,1)} %param.14), kind=kOutput, calls=%fused_computation.28 | convolution fusion | flops 2149056512 | bytes 11534336 | tf_op jit(solution)/shard_map/dot_general | solution.py:142
  360.6 1.9 copy.69
  362.5 2.3 broadcast_multiply_fusion.1
  364.9 2.3 broadcast_multiply_fusion
  367.2 4.1 fusion.10
  371.2 2.8 slice_bitcast_fusion
  374.1 31.9 %while.22 = (s32[]{:T(128)}, f32[8,64,128]{2,1,0:T(8,128)S(1)}, f32[8,8]{1,0:T(8,128)S(1)}, f32[8,8,64,64]{3,2,0,1:T(8,128)}, f32[8,8,64,64]{3,2,0,1:T(8,128)}, /*index=5*/f32[8,8,64,64]{3,2,0,1:T(8,128)}, s32[]{:T(128)}) while((s32[]{:T(128)}, f32[8,64,128]{2,1,0:T(8,128)S(1)}, f32[8,8]{1,0:T(8,128)S(1)}, f32[8,8,64,64]{3,2,0,1:T(8,128)}, ...), condition=%wide.region_3.4_spmd, body=%wide.region_2.3_spmd.sunk | while | flops 100859904 | bytes 2229429 | solution.py:119
  375.1 1.3 convolution_subtract_fusion.2
  376.5 1.6 convolution_add_fusion.2
  379.1 1.3 convolution_subtract_fusion.2
  380.4 1.6 convolution_add_fusion.2
  383.1 1.3 convolution_subtract_fusion.2
  384.4 1.6 convolution_add_fusion.2
  388.4 1.6 convolution_add_fusion.2
  392.4 1.6 convolution_add_fusion.2
  395.0 1.3 convolution_subtract_fusion.2
  396.4 1.6 convolution_add_fusion.2
  400.4 1.6 convolution_add_fusion.2
  404.3 1.6 convolution_add_fusion.2
  406.8 89.1 %all-gather.3.cloned.1.call-done = f32[32,4,64,64]{3,2,1,0:T(8,128)} async-done(((f32[2,4,64,64]{3,2,1,0:T(8,128)}), f32[32,4,64,64]{3,2,1,0:T(8,128)}) %all-gather.3.cloned.1.call-update) | async-done | bytes 2097168 | tf_op jit(solution)/shard_map/all_gather | solution.py:18
  495.9 24.2 %while.23 = (s32[]{:T(128)}, f32[2,4,64,64]{2,3,1,0:T(8,128)S(1)}, s32[]{:T(128)}, f32[16,2,4,64,64]{4,3,2,1,0:T(8,128)}, s32[]{:T(128)}, /*index=5*/s32[]{:T(128)}, s32[]{:T(128)}, s32[]{:T(128)}) while((s32[]{:T(128)}, f32[2,4,64,64]{2,3,1,0:T(8,128)S(1)}, s32[]{:T(128)}, f32[16,2,4,64,64]{4,3,2,1,0:T(8,128)}, s32[]{:T(128)}, ...), condition=%wide.region_5.6_spmd, body=%wide.region_4.5_spmd.sunk | while | flops 25165828 | bytes 786567 | solution.py:25
  496.0 1.6 convolution_bitcast_fusion.2
  497.6 1.6 convolution_bitcast_fusion.2
  499.2 1.6 convolution_bitcast_fusion.2
  500.8 1.6 convolution_bitcast_fusion.2
  502.4 1.6 convolution_bitcast_fusion.2
  504.1 1.6 convolution_bitcast_fusion.2
  505.7 1.6 convolution_bitcast_fusion.2
  507.3 1.6 convolution_bitcast_fusion.2
  508.9 1.6 convolution_bitcast_fusion.2
  510.5 1.6 convolution_bitcast_fusion.2
  512.1 1.6 convolution_bitcast_fusion.2
  513.7 1.6 convolution_bitcast_fusion.2
  515.3 1.6 convolution_bitcast_fusion.2
  516.9 1.6 convolution_bitcast_fusion.2
  518.6 1.6 convolution_bitcast_fusion.2
  521.8 4.0 all-to-all-start
  525.9 12.5 %all-to-all-done = f32[16,1,2048]{2,1,0:T(1,128)S(1)} async-done(((f32[16,1,2048]{2,1,0:T(1,128)}), f32[16,1,2048]{2,1,0:T(1,128)S(1)}, u32[]{:S(2)}, u32[]{:S(2)}) %all-to-all-start) | async-done | bytes 131104 | tf_op jit(solution)/shard_map/all_to_all | solution.py:36
  541.0 4.3 all-to-all-start.1
  545.9 11.8 %all-to-all-done.1 = f32[16,1,512]{2,1,0:T(1,128)S(1)} async-done(((f32[16,1,512]{2,1,0:T(1,128)}), f32[16,1,512]{2,1,0:T(1,128)S(1)}, u32[]{:S(2)}, u32[]{:S(2)}) %all-to-all-start.1) | async-done | bytes 32800 | tf_op jit(solution)/shard_map/all_to_all | solution.py:42
  (85 shorter events, 23.8 us)
Async XLA Ops:
  7.2 14.6 %copy-start = (bf16[4096,256]{1,0:T(8,128)(2,1)S(1)}, bf16[4096,256]{1,0:T(8,128)(2,1)}, u32[]{:S(2)}) copy-start(bf16[4096,256]{1,0:T(8,128)(2,1)} %param.13) | copy-start | bytes 6291460
  7.2 488.7 %all-gather.3.cloned.1.call-start = ((), (), s32[]{:S(2)}) async-start(), calls=%async_computation.2 | async-start | bytes 4456448 | tf_op jit(solution)/shard_map/all_gather | solution.py:18
  32.0 1.4 copy-start.3
  362.5 2.4 copy-start.4
  364.9 2.3 copy-start.5
  406.0 0.7 copy-start.1
  495.9 24.2 %copy-start.2 = (f32[8,64,128]{2,1,0:T(8,128)S(1)}, f32[8,64,128]{2,1,0:T(8,128)}, u32[]{:S(2)}) copy-start(f32[8,64,128]{2,1,0:T(8,128)} %copy-done.1) | copy-start | bytes 786436
  495.9 29.8 %copy-start.6 = (bf16[2,256]{1,0:T(2,128)(2,1)S(1)}, bf16[2,256]{1,0:T(2,128)(2,1)}, u32[]{:S(2)}) copy-start(bf16[2,256]{1,0:T(2,128)(2,1)} %param.19) | copy-start | bytes 3076
  521.8 16.6 %all-to-all-start = ((f32[16,1,2048]{2,1,0:T(1,128)}), f32[16,1,2048]{2,1,0:T(1,128)S(1)}, u32[]{:S(2)}, u32[]{:S(2)}) async-start(f32[16,1,2048]{2,1,0:T(1,128)} %reshape.84), calls=%async_computation | async-start | bytes 262144 | tf_op jit(solution)/shard_map/all_to_all | solution.py:36
  541.0 16.7 %all-to-all-start.1 = ((f32[16,1,512]{2,1,0:T(1,128)}), f32[16,1,512]{2,1,0:T(1,128)S(1)}, u32[]{:S(2)}, u32[]{:S(2)}) async-start(f32[16,1,512]{2,1,0:T(1,128)} %reshape.86), calls=%async_computation.1 | async-start | bytes 65536 | tf_op jit(solution)/shard_map/all_to_all | solution.py:42
Sparse Core Ops, SparseCore 0:
  406.8 89.0 all-gather.2
where the time goes:
time: 569 us; the launch traced here: 566 us
  other arithmetic  328 us (58%)
  waiting for transfers between devices  113 us (20%)
  matrix products  80.4 us (14%)
  local copies, waits for them, and re-layouts  20.7 us (4%)
  between operations  14.3 us (3%)
  starting transfers between devices  8.31 us (1%)
    another operation x1, other arithmetic, block_parts(): solved = jax.scipy.linalg.solve_triangular(lower, right, lower=True)  316 us
    all_gather x1, waiting for transfers between devices, prefix(): gathered = lax.all_gather(part, axis)  89.1 us
    dot_general x16, matrix products, matmul(): return jnp.einsum('shij,shjk->shik', left, right, precision=finest)  24 us
    dot_general x8, matrix products, advance(): jnp.einsum('gck,gcw->gkw', carried, fresh, precision=finest)  12.9 us
    all_to_all x1, waiting for transfers between devices, sent_and_summed(): lax.all_to_all(pieces, axis, split_axis=0, concat_axis=0, tiled=True)  12.5 us
    all_to_all x1, waiting for transfers between devices, sent_to_all(): lax.all_to_all(jnp.broadcast_to(x[None], (size, *x.shape)), axis, 0, 0, t...  11.8 us
  transfers between devices with their start and end apart: 3, of which 3 were waited for; matrix products, arithmetic and copies ran while one was open for 0% of the time, Pallas kernels for 0%

commit v1 on v0

v1 whole, which is shorter than its diff:
```python
import functools

import jax
import jax.numpy as jnp
from jax import lax
from jax.experimental import pallas as pl
from jax.experimental.pallas import tpu as pltpu
from jax.sharding import PartitionSpec as P

HEAD = 64
BASE = 8
F32 = jnp.float32
BF16 = jnp.bfloat16


def iota(shape, dim):
    return lax.broadcasted_iota(jnp.int32, shape, dim)


def silu(v):
    return v / (1.0 + jnp.exp(-v))


def dot(a, b, dims=(1, 0)):
    return lax.dot_general(a, b, (((dims[0],), (dims[1],)), ((), ())), preferred_element_type=F32)


def lanes_turned(x, amount):
    amount %= x.shape[1]
    return pltpu.roll(x, amount, 1) if amount else x


def block_diagonal(x, mask):
    return jnp.tile(x, (mask.shape[0] // x.shape[0], 1)) * mask


def running_sum(x):
    rows = iota(x.shape, 0)
    step = 1
    while step < x.shape[0]:
        x = x + jnp.where(rows >= step, pltpu.roll(x, step, 0), 0.0)
        step *= 2
    return x


def small_inverse(lower, heads):
    width = lower.shape[1]
    column = iota((BASE, width), 1) % HEAD
    blocks = jnp.zeros((BASE, width), F32)
    for r in range(HEAD // BASE):
        blocks = jnp.where(column // BASE == r, lower[BASE * r : BASE * (r + 1)], blocks)
    inverse = jnp.where(iota((BASE, width), 0) == column % BASE, 1.0, 0.0)
    lane = iota((BASE, 128), 1)
    pieces = []
    for first in range(0, width, 128):
        part, x = blocks[:, first : first + 128], inverse[:, first : first + 128]
        for m in range(BASE - 1):
            factor = jnp.take_along_axis(part, lane // BASE * BASE + m, axis=1)
            x = x - factor * x[m : m + 1]
        pieces.append(x)
    inverse = jnp.concatenate(pieces, axis=1)
    return jnp.concatenate(
        [jnp.where(column // BASE == r, inverse, 0.0) for r in range(HEAD // BASE)], axis=0
    )


def chunk_map(k, v, beta, total, mask, heads):
    width = heads * HEAD
    row, column = iota((HEAD, width), 0), iota((HEAD, width), 1) % HEAD
    eye = row == column
    across = jnp.sum(jnp.where(eye, total, 0.0), axis=0, keepdims=True)
    last = total[HEAD - 1 :]
    low = k.astype(BF16)
    gram = dot(low, block_diagonal(low, mask), (1, 1))
    lower = jnp.where(row > column, beta * gram * jnp.exp(jnp.minimum(total - across, 0.0)), 0.0)
    inverse = small_inverse(lower, heads)
    size = BASE
    while size < HEAD:
        here = (row // (2 * size) == column // (2 * size)) & (row // size > column // size)
        off = jnp.where(here, lower, 0.0).astype(BF16)
        rounded = inverse.astype(BF16)
        inner = dot(off, block_diagonal(rounded, mask))
        inverse = inverse - dot(rounded, block_diagonal(inner.astype(BF16), mask))
        size *= 2
    carried = k * jnp.exp(last - total)
    turned = carried.T
    turned = jnp.concatenate(
        [turned[HEAD * h : HEAD * (h + 1)] for h in range(heads)], axis=1
    ).astype(BF16)
    closing = dot(turned, block_diagonal(inverse.astype(BF16), mask)).astype(BF16)
    taken = (k * (beta * jnp.exp(total))).astype(BF16)
    added = (v * beta).astype(BF16)
    removal = dot(closing, block_diagonal(taken, mask))
    removal = removal + jnp.where(eye, 1.0 - jnp.exp(last), 0.0)
    return removal, dot(closing, block_diagonal(added, mask))


def after(later, earlier, mask):
    r2, o2 = later
    r1, o1 = earlier
    low = r2.astype(BF16)
    return (
        r1 + r2 - dot(low, block_diagonal(r1.astype(BF16), mask)),
        o1 + o2 - dot(low, block_diagonal(o1.astype(BF16), mask)),
    )


def composed(parts, combine):
    while len(parts) > 1:
        joined = [combine(parts[i + 1], parts[i]) for i in range(0, len(parts) - 1, 2)]
        parts = joined + parts[len(joined) * 2 :]
    return parts[0]


def local_kernel(
    heads, seqs, length, place_ref, speed_ref, x_ref, wk_ref, wv_ref, wb_ref, wf_ref, extra_ref, out_ref,
    kv_acc, small_acc, mask_ref, k_ref, v_ref, beta_ref, total_ref
):
    step = pl.program_id(0)
    width = heads * HEAD
    all_heads = wb_ref.shape[1]

    @pl.when(step == 0)
    def _():
        kv_acc[...] = jnp.zeros_like(kv_acc)
        small_acc[...] = jnp.zeros_like(small_acc)

    x = x_ref[...]
    kv_acc[:, :width] += dot(x, wk_ref[...])
    kv_acc[:, width:] += dot(x, wv_ref[...])
    small_acc[...] += dot(x, jnp.concatenate([wb_ref[...], wf_ref[...]], axis=1))

    @pl.when(step == pl.num_programs(0) - 1)
    def _():
        rows, cols = iota((width, width), 0), iota((width, width), 1)
        mask_ref[...] = jnp.where(rows // HEAD == cols // HEAD, 1.0, 0.0).astype(BF16)
        mask = mask_ref[...]
        first = place_ref[0] * heads
        pick_row, pick_col = iota((2 * all_heads, width), 0), iota((2 * all_heads, width), 1)
        pick_b = jnp.where(pick_row == first + pick_col // HEAD, 1.0, 0.0).astype(BF16)
        pick_f = jnp.where(pick_row == all_heads + first + pick_col // HEAD, 1.0, 0.0).astype(BF16)
        spread = jnp.where(iota((heads, width), 0) == iota((heads, width), 1) // HEAD, 1.0, 0.0).astype(BF16)
        lane_head = iota((1, width), 1) // HEAD
        speed = jnp.zeros((1, width), F32)
        for h in range(heads):
            speed = jnp.where(lane_head == h, speed_ref[h], speed)
        rate = jnp.exp(speed)
        count = seqs * length // HEAD

        def prepare(n, carry):
            here = pl.ds(pl.multiple_of(n * HEAD, HEAD), HEAD)
            keys = silu(kv_acc[here, :width].astype(BF16).astype(F32))
            squares = keys * keys
            high = squares.astype(BF16)
            rest = (squares - high.astype(F32)).astype(BF16)
            norm = dot(high, mask) + dot(rest, mask)
            k_ref[here] = keys * lax.rsqrt(norm + 1e-06)
            v_ref[here] = silu(kv_acc[here, width:].astype(BF16).astype(F32))
            small = small_acc[here].astype(BF16)
            beta_ref[here] = 1.0 / (1.0 + jnp.exp(-dot(small, pick_b)))
            pre = dot(small, pick_f)
            soft = jnp.maximum(pre, 0.0) + jnp.log1p(jnp.exp(-jnp.abs(pre)))
            gamma = dot(extra_ref[here], spread) - rate * soft
            total_ref[here] = running_sum(gamma)
            return carry

        lax.fori_loop(0, count, prepare, 0)
        lane = iota((HEAD // 2, 128), 1)
        quarter_lane = iota((HEAD // 4, 128), 1)
        for s in range(seqs):
            parts = []
            for c in range(length // HEAD):
                here = pl.ds(s * length + c * HEAD, HEAD)
                parts.append(
                    chunk_map(k_ref[here], v_ref[here], beta_ref[here], total_ref[here], mask, heads)
                )
            removal, offset = composed(parts, lambda b, a: after(b, a, mask))
            for pair in range(heads // 2):
                r = removal[:, 128 * pair : 128 * (pair + 1)]
                o = offset[:, 128 * pair : 128 * (pair + 1)]
                top, bottom = r[: HEAD // 2], r[HEAD // 2 :]
                even = jnp.where(lane < HEAD, top, lanes_turned(bottom, HEAD))
                odd = jnp.where(lane < HEAD, lanes_turned(top, HEAD), bottom)
                for d in range(4):
                    dest = (s * heads + 2 * pair) * 2 + d
                    out_ref[dest, : HEAD // 2] = even if d < 2 else odd
                    packed = jnp.zeros((HEAD // 4, 128), F32)
                    for q in range(4):
                        piece = o[HEAD // 4 * q : HEAD // 4 * (q + 1)]
                        packed = jnp.where(quarter_lane // 32 == q, lanes_turned(piece, 32 * (q - d)), packed)
                    out_ref[dest, HEAD // 2 :] = packed


def owner_kernel(sources, q_ref, in_ref, out_ref, state_ref):
    lane = iota((HEAD, 128), 1)
    parts = []
    for i in range(sources):
        r, o = in_ref[i, : HEAD // 2], in_ref[i, HEAD // 2 :]
        left = jnp.concatenate([r, lanes_turned(r, HEAD)], axis=0)
        right = jnp.concatenate([lanes_turned(o, HEAD - 32 * q) for q in range(4)], axis=0)
        parts.append(jnp.where(lane < HEAD, left, jnp.where(lane < HEAD + 32, right, 0.0)))

    def combine(later, earlier):
        removal = jnp.where(lane < HEAD, later, 0.0)
        high = removal.astype(BF16)
        low = (removal - high.astype(F32)).astype(BF16)
        e_high = earlier.astype(BF16)
        e_low = (earlier - e_high.astype(F32)).astype(BF16)
        both = jnp.concatenate([e_high, e_high], axis=0)
        mixed = jnp.concatenate([e_low, e_low], axis=0)
        product = dot(high, both) + dot(high, mixed) + dot(low, both)
        return earlier + later - product

    final = composed(parts, combine)
    state_ref[...] = lanes_turned(final, HEAD)
    lane16 = iota((HEAD // 4, 128), 1)
    rows = jnp.zeros((HEAD // 4, 128), F32)
    for a in range(4):
        piece = state_ref[pl.ds(a, HEAD // 4, stride=4), :]
        rows = jnp.where(lane16 // 32 == a, lanes_turned(piece, 32 * a), rows)
    out_ref[:, :128] = rows
    state = state_ref[...]
    q = q_ref[...].astype(BF16)
    read = jnp.zeros((8, 128), F32)
    for _ in range(3):
        piece = state.astype(BF16)
        read = read + dot(q, piece)
        state = state - piece.astype(F32)
    out_ref[:, 128:] = jnp.broadcast_to(read[:1], (HEAD // 4, 128))


def body(
    layer_feed,
    address_mapping,
    content_mapping,
    beta_mapping_matrix,
    forgetting_mapping,
    logged_fading_speed,
    extra_forgetting,
    opening_probe,
):
    seqs, length, depth = layer_feed.shape
    width = address_mapping.shape[1]
    heads = width // HEAD
    all_heads = beta_mapping_matrix.shape[1]
    tokens = seqs * length
    ways = lax.axis_size("sp")
    steps = 8
    deep = depth // steps
    place = lax.axis_index("tp").astype(jnp.int32).reshape(1)
    whole = lambda i: (0, 0)
    maps = pl.pallas_call(
        functools.partial(local_kernel, heads, seqs, length),
        grid=(steps,),
        out_shape=jax.ShapeDtypeStruct((ways, 48, 128), F32),
        in_specs=[
            pl.BlockSpec(memory_space=pltpu.SMEM),
            pl.BlockSpec(memory_space=pltpu.SMEM),
            pl.BlockSpec((tokens, deep), lambda i: (0, i)),
            pl.BlockSpec((deep, width), lambda i: (i, 0)),
            pl.BlockSpec((deep, width), lambda i: (i, 0)),
            pl.BlockSpec((deep, all_heads), lambda i: (i, 0)),
            pl.BlockSpec((deep, all_heads), lambda i: (i, 0)),
            pl.BlockSpec((tokens, heads), whole),
        ],
        out_specs=pl.BlockSpec((ways, 48, 128), lambda i: (0, 0, 0)),
        scratch_shapes=[
            pltpu.VMEM((tokens, 2 * width), F32),
            pltpu.VMEM((tokens, 2 * all_heads), F32),
            pltpu.VMEM((width, width), BF16),
            pltpu.VMEM((tokens, width), F32),
            pltpu.VMEM((tokens, width), F32),
            pltpu.VMEM((tokens, width), F32),
            pltpu.VMEM((tokens, width), F32),
        ],
        compiler_params=pltpu.CompilerParams(vmem_limit_bytes=48 << 20),
        name="local_maps",
    )(
        place,
        logged_fading_speed,
        layer_feed.reshape(tokens, depth),
        address_mapping,
        content_mapping,
        beta_mapping_matrix,
        forgetting_mapping,
        extra_forgetting.reshape(tokens, heads),
    )
    got = lax.all_to_all(maps, "sp", 0, 0, tiled=True)
    group = lax.axis_index("sp") // 2
    query = lax.dynamic_slice_in_dim(opening_probe.reshape(seqs * heads, HEAD), group, 1, 0).astype(F32)
    query = jnp.pad(jnp.broadcast_to(query, (8, HEAD)), ((0, 0), (0, 0)))
    shares = pl.pallas_call(
        functools.partial(owner_kernel, ways),
        out_shape=jax.ShapeDtypeStruct((ways, 256), F32),
        scratch_shapes=[pltpu.VMEM((HEAD, 128), F32)],
        name="owner_state",
    )(query, got)
    mine = lax.all_to_all(shares.reshape(ways, 1, 256), "sp", 0, 0, tiled=True).reshape(ways, 256)
    rows = mine[:, :128].reshape(seqs * heads, 2, 4, 32).transpose(0, 2, 1, 3)
    context_memory_tensor = rows.reshape(seqs, heads, 4, HEAD).astype(BF16)
    read = mine[:, 128:160].reshape(seqs, heads, HEAD)
    read = read * lax.rsqrt(jnp.mean(read * read, axis=-1, keepdims=True) + 1e-06)
    return context_memory_tensor, read.reshape(seqs, width).astype(BF16)


def solution(mesh):
    in_specs = (
        P("grp", "sp", None),
        P(None, "tp"),
        P(None, "tp"),
        P(),
        P(),
        P("tp"),
        P("grp", "sp", "tp"),
        P("grp", "tp"),
    )
    out_specs = (P("grp", "tp", "sp", None), P("grp", "tp"))
    return jax.shard_map(body, mesh=mesh, in_specs=in_specs, out_specs=out_specs, check_vma=False)
```

time: 569 us -> 118 us (0.21)
  other arithmetic: 328 us -> 0.67 us
  waiting for transfers between devices: 113 us -> 23.6 us
  matrix products: 80.4 us -> 0 us
  Pallas kernels: 0 us -> 42 us
  blocking collectives: 0 us -> 18.2 us
  starting transfers between devices: 8.31 us -> 24 us
  between operations: 14.3 us -> 0.73 us
  local copies, waits for them, and re-layouts: 20.7 us -> 8.03 us
    another operation x2 -> x0, other arithmetic: 318 us -> none  [the longest x1 316 us: block_parts(): solved = jax.scipy.linalg.solve_triangular(lower, right, lower=True)]
    all_gather x1 -> x0, waiting for transfers between devices: 89.1 us -> none  [prefix(): gathered = lax.all_gather(part, axis)]
    dot_general x38 -> x0, matrix products: 76.4 us -> none  [the longest x16 24 us: matmul(): return jnp.einsum('shij,shjk->shik', left, right, precision=finest)]
    pallas_call x0 -> x2, Pallas kernels: none -> 42 us  [the longest x1 39.3 us: body(): pl.pallas_call(functools.partial(local_kernel, heads, seqs, length), grid...]
    all_to_all x0 -> x1, blocking collectives: none -> 18.2 us  [body(): lax.all_to_all(shares.reshape(ways, 1, 256), 'sp', 0, 0, tiled=True)]
    all_to_all x2 -> x1, starting transfers between devices: 8.25 us -> 24 us  [body(): got = lax.all_to_all(maps, 'sp', 0, 0, tiled=True)]
    squeeze x8 -> x0, local copies, waits for them, and re-layouts: 7.81 us -> none  [run_blocks(): final, _ = lax.scan(advance, start, moved)]
    mul x4 -> x1, other arithmetic: 6.91 us -> 0.01 us  [body(): read * read]
  transfers between devices with their start and end apart: 3 -> 1, of which waited for: 3 -> 1; matrix products, arithmetic and copies ran while one was open for 0% -> 0% of each run, Pallas kernels for 0% -> 0%
where the time goes in v1:
time: 118 us; the launch traced here: 117 us
  Pallas kernels  42 us (36%)
  starting transfers between devices  24 us (20%)
  waiting for transfers between devices  23.6 us (20%)
  blocking collectives  18.2 us (15%)
  local copies, waits for them, and re-layouts  8.03 us (7%)
    pallas_call x1, Pallas kernels, body(): pl.pallas_call(functools.partial(local_kernel, heads, seqs, length), grid...  39.3 us
    all_to_all x1, starting transfers between devices, body(): got = lax.all_to_all(maps, 'sp', 0, 0, tiled=True)  24 us
    all_to_all x1, waiting for transfers between devices, body(): got = lax.all_to_all(maps, 'sp', 0, 0, tiled=True)  23.6 us
    all_to_all x1, blocking collectives, body(): lax.all_to_all(shares.reshape(ways, 1, 256), 'sp', 0, 0, tiled=True)  18.2 us
    unnamed x12, local copies, waits for them, and re-layouts  5.49 us
    pallas_call x1, Pallas kernels, body(): pl.pallas_call(functools.partial(owner_kernel, ways), out_shape=jax.Shape...  2.7 us
  transfers between devices with their start and end apart: 1, of which 1 were waited for; matrix products, arithmetic and copies ran while one was open for 0% of the time, Pallas kernels for 0%

profile of v1, /device:TPU:46, one launch (start us, length us, event | category | flops | bytes accessed | tf_op | source)
XLA Modules:
  0.0 117.3 jit_solution(15144984433075027606)
XLA Ops:
  0.6 0.0 copy-start.1
  0.6 0.9 copy.14
  1.5 1.4 %copy.15.wb_ref = bf16[4096,32]{1,0:T(8,128)(2,1)S(1)} copy(bf16[4096,32]{0,1:T(8,128)(2,1)} %param.11) | data formatting | bytes 524288 | tf_op args[3]
  3.0 1.4 %copy.16.wf_ref = bf16[4096,32]{1,0:T(8,128)(2,1)S(1)} copy(bf16[4096,32]{0,1:T(8,128)(2,1)} %param.12) | data formatting | bytes 524288 | tf_op args[4]
  4.4 0.0 copy-done.1
  4.4 0.0 copy-start
  4.4 1.6 %copy-done = bf16[4096,256]{1,0:T(8,128)(2,1)S(1)} copy-done((bf16[4096,256]{1,0:T(8,128)(2,1)S(1)}, bf16[4096,256]{1,0:T(8,128)(2,1)}, u32[]{:S(2)}) %copy-start) | copy-done | bytes 2097176
  6.0 0.0 copy-start.3
  6.0 39.3 %local_maps.1 = f32[16,48,128]{2,1,0:T(8,128)} custom-call(s32[1]{0:T(128)} %bitcast.1.place_ref, f32[4]{0:T(128)S(1)} %copy-done.1, bf16[1024,4096]{1,0:T(8,128)(2,1)} %bitcast.12, bf16[4096,256]{1,0:T(8,128)(2,1)S(1)} %copy-done, bf16[4096,256]{1,0:T(8,128)(2,1)} %wv_ref.1, bf16[4096,32]{1,0:T(8,128)(2,1)S(1)} %copy.15.wb_ref, ...), custom_call_target="tpu_custom_call" | custom-call | tf_op jit(solution)/shard_map/local_maps/pallas_call | solution.py:252
  45.3 24.0 %all-to-all-start = ((f32[16,48,128]{2,1,0:T(8,128)}), f32[16,48,128]{2,1,0:T(8,128)S(1)}, u32[]{:S(2)}, u32[]{:S(2)}) async-start(f32[16,48,128]{2,1,0:T(8,128)} %local_maps.1), calls=%async_computation | async-start | bytes 786432 | tf_op jit(solution)/shard_map/all_to_all | solution.py:288
  69.3 0.0 copy-done.3
  69.3 0.1 reshape.41
  69.4 23.6 %all-to-all-done.in_ref = f32[16,48,128]{2,1,0:T(8,128)S(1)} async-done(((f32[16,48,128]{2,1,0:T(8,128)}), f32[16,48,128]{2,1,0:T(8,128)S(1)}, u32[]{:S(2)}, u32[]{:S(2)}) %all-to-all-start) | async-done | bytes 393248 | tf_op jit(solution)/shard_map/all_to_all | solution.py:288
  93.0 0.0 copy-start.2
  93.0 0.6 broadcast_in_dim.13.q_ref
  93.7 0.1 copy-done.2
  93.8 2.7 %owner_state.1 = f32[16,256]{1,0:T(8,128)} custom-call(f32[8,64]{1,0:T(8,128)} %broadcast_in_dim.13.q_ref, f32[16,48,128]{2,1,0:T(8,128)} %copy-done.2), custom_call_target="tpu_custom_call" | custom-call | tf_op jit(solution)/shard_map/owner_state/pallas_call | solution.py:292
  96.5 0.7 copy.17
  97.2 18.2 %all_to_all.10 = f32[16,1,256]{2,1,0:T(1,128)S(1)} all-to-all(f32[16,1,256]{2,1,0:T(1,128)S(1)} %copy.17), channel_id=1, replica_groups=mesh['grp'=2,'sp'=16,'tp'=8] {'sp'}, dimensions={0} | all-to-all | bytes 32768 | tf_op jit(solution)/shard_map/all_to_all | solution.py:298
  115.5 0.1 mul.18
  115.6 0.1 reduce_sum.9
  115.7 0.1 reshape.47
  115.7 0.1 mul.19
  115.8 0.1 mul.20
  115.9 0.1 convert_element_type.14
  116.0 0.7 convert_element_type.16
  116.7 0.6 multiply_convert_fusion
  (6 shorter events, 0.0 us)
Async XLA Ops:
  0.6 3.8 %copy-start.1 = (f32[4]{0:T(128)S(1)}, f32[4]{0:T(128)}, u32[]{:S(2)}) copy-start(f32[4]{0:T(128)} %speed_ref.1) | copy-start | bytes 52
  4.4 1.6 %copy-start = (bf16[4096,256]{1,0:T(8,128)(2,1)S(1)}, bf16[4096,256]{1,0:T(8,128)(2,1)}, u32[]{:S(2)}) copy-start(bf16[4096,256]{1,0:T(8,128)(2,1)} %wk_ref.1) | copy-start | bytes 6291460
  6.0 63.3 %copy-start.3 = (bf16[2,256]{1,0:T(2,128)(2,1)S(1)}, bf16[2,256]{1,0:T(2,128)(2,1)}, u32[]{:S(2)}) copy-start(bf16[2,256]{1,0:T(2,128)(2,1)} %param.15) | copy-start | bytes 3076
  45.3 47.7 %all-to-all-start = ((f32[16,48,128]{2,1,0:T(8,128)}), f32[16,48,128]{2,1,0:T(8,128)S(1)}, u32[]{:S(2)}, u32[]{:S(2)}) async-start(f32[16,48,128]{2,1,0:T(8,128)} %local_maps.1), calls=%async_computation | async-start | bytes 786432 | tf_op jit(solution)/shard_map/all_to_all | solution.py:288
  93.0 0.8 copy-start.2

commit v2 on v1

v2 whole, which is shorter than its diff:
```python
import functools

import jax
import jax.numpy as jnp
from jax import lax
from jax.experimental import pallas as pl
from jax.experimental.pallas import tpu as pltpu
from jax.sharding import PartitionSpec as P

HEAD = 64
BASE = 8
F32 = jnp.float32
BF16 = jnp.bfloat16


def iota(shape, dim):
    return lax.broadcasted_iota(jnp.int32, shape, dim)


def silu(v):
    return v / (1.0 + jnp.exp(-v))


def dot(a, b, dims=(1, 0)):
    return lax.dot_general(a, b, (((dims[0],), (dims[1],)), ((), ())), preferred_element_type=F32)


def lanes_turned(x, amount):
    amount %= x.shape[1]
    return pltpu.roll(x, amount, 1) if amount else x


def block_diagonal(x, mask):
    return jnp.tile(x, (mask.shape[0] // x.shape[0], 1)) * mask


def summed_from(x, direction):
    place = iota(x.shape, 1) % HEAD
    if direction < 0:
        place = HEAD - 1 - place
    step = 1
    while step < HEAD:
        x = x + jnp.where(place >= step, lanes_turned(x, direction * step), 0.0)
        step *= 2
    return x


def pieces_of(x, count):
    pieces = []
    for _ in range(count):
        piece = x.astype(BF16).astype(F32)
        pieces.append(piece)
        x = x - piece
    return pieces


def chunk_row(x, n, heads):
    here = x[:, 128 * (n // 2) : 128 * (n // 2 + 1)]
    turned = lanes_turned(here, HEAD)
    left, right = (here, turned) if n % 2 == 0 else (turned, here)
    first = iota((1, 128), 1) < HEAD
    return jnp.concatenate(
        [jnp.where(first, left[h : h + 1], right[h + 1 : h + 2]) for h in range(0, heads, 2)], axis=1
    )


def small_inverse(lower):
    width = lower.shape[1]
    block = iota((BASE, width), 1) % HEAD // BASE
    blocks = lower[:BASE]
    for r in range(1, HEAD // BASE):
        blocks = jnp.where(block == r, lower[BASE * r : BASE * (r + 1)], blocks)
    lane = iota((BASE, 128), 1)
    pieces = []
    for first in range(0, width, 128):
        part = blocks[:, first : first + 128]
        x = jnp.where(iota((BASE, 128), 0) == lane % BASE, 1.0, 0.0)
        for m in range(BASE - 1):
            factor = jnp.take_along_axis(part, lane // BASE * BASE + m, axis=1)
            x = x - factor * x[m : m + 1]
        pieces.append(x)
    inverse = jnp.concatenate(pieces, axis=1)
    return jnp.concatenate([jnp.where(block == r, inverse, 0.0) for r in range(HEAD // BASE)], axis=0)


def after(later, earlier, mask):
    high, low = pieces_of(later[0], 2)
    both = jnp.concatenate([high, low], axis=0).astype(BF16)
    joined = []
    for second, first in zip(later, earlier):
        first_high, first_low = pieces_of(first, 2)
        product = dot(both, block_diagonal(first_high.astype(BF16), mask))
        rest = dot(both[:HEAD], block_diagonal(first_low.astype(BF16), mask))
        joined.append(first + second - (product[:HEAD] + product[HEAD:] + rest))
    return tuple(joined)


def composed(parts, combine):
    while len(parts) > 1:
        joined = [combine(parts[i + 1], parts[i]) for i in range(0, len(parts) - 1, 2)]
        parts = joined + parts[len(joined) * 2 :]
    return parts[0]


def local_kernel(
    heads, place_ref, speed_ref, x_ref, wk_ref, wv_ref, wb_ref, wf_ref, extra_ref, out_ref,
    kv_acc, small_acc, wide_ref, k_ref, low_ref, taken_ref, added_ref, lower_ref, inverse_ref, inner_ref
):
    step = pl.program_id(0)
    width = heads * HEAD
    seqs, length, deep = x_ref.shape
    tokens = seqs * length
    all_heads = wb_ref.shape[0]

    @pl.when(step == 0)
    def _():
        kv_acc[...] = jnp.zeros_like(kv_acc)
        small_acc[...] = jnp.zeros_like(small_acc)

    x = x_ref[...].reshape(tokens, deep)
    kv_acc[:, :width] += dot(x, wk_ref[...])
    kv_acc[:, width:] += dot(x, wv_ref[...])
    small_acc[...] += dot(jnp.concatenate([wb_ref[...], wf_ref[...]], axis=0), x, (1, 1))

    @pl.when(step == pl.num_programs(0) - 1)
    def _():
        rows, cols = iota((width, width), 0), iota((width, width), 1)
        mask = jnp.where(rows // HEAD == cols // HEAD, 1.0, 0.0).astype(BF16)
        first = place_ref[0] * heads
        half = 2 * heads
        head_of_row = iota((half, 2 * all_heads), 0) % heads
        column = iota((half, 2 * all_heads), 1)
        small = small_acc[...].astype(BF16)
        beta_pre = dot(jnp.where(column == first + head_of_row, 1.0, 0.0).astype(BF16), small)
        decay_pre = dot(jnp.where(column == all_heads + first + head_of_row, 1.0, 0.0).astype(BF16), small)
        twice = jnp.where(iota((half, heads), 0) % heads == iota((half, heads), 1), 1.0, 0.0).astype(BF16)
        extra = jnp.concatenate([dot(twice, extra_ref[s]) for s in range(seqs)], axis=1)
        row_head = iota((half, 1), 0) % heads
        speed = jnp.zeros((half, 1), F32)
        for h in range(heads):
            speed = jnp.where(row_head == h, speed_ref[h], speed)
        soft = jnp.maximum(decay_pre, 0.0) + jnp.log1p(jnp.exp(-jnp.abs(decay_pre)))
        gamma = extra - jnp.exp(speed) * soft
        beta = 1.0 / (1.0 + jnp.exp(-beta_pre))
        total = summed_from(gamma, 1)
        last_lane = iota(gamma.shape, 1) % HEAD == HEAD - 1
        rest = summed_from(jnp.where(last_lane, 0.0, lanes_turned(gamma, -1)), -1)
        taking = beta * jnp.exp(total)
        carry = jnp.exp(rest)
        dropped = 1.0 - jnp.exp(total + rest)
        stack = pieces_of(beta, 2) + pieces_of(total, 3) + pieces_of(taking, 2)
        owner = [0] * 2 + [1] * 3 + [2] * 2
        pick_row, pick_col = iota((half * len(stack), 3 * width), 0), iota((half * len(stack), 3 * width), 1)
        kind = jnp.zeros(pick_row.shape, jnp.int32)
        for i, q in enumerate(owner):
            kind = jnp.where(pick_row // half == i, q, kind)
        pick = jnp.where((pick_col // width == kind) & (pick_row % half == pick_col % width // HEAD), 1.0, 0.0)
        wide_ref[...] = dot(jnp.concatenate(stack, axis=0).astype(BF16).T, pick.astype(BF16))

        count = tokens // HEAD
        for n in range(0, tokens, 256):
            here = pl.ds(n, 256)
            keys = silu(kv_acc[here, :width].astype(BF16).astype(F32))
            high, low = pieces_of(keys * keys, 2)
            norm = dot(high.astype(BF16), mask) + dot(low.astype(BF16), mask)
            keys = keys * lax.rsqrt(norm + 1e-06)
            k_ref[here] = keys
            low_ref[here] = keys.astype(BF16)
            taken_ref[here] = (keys * wide_ref[here, 2 * width :]).astype(BF16)
            values = silu(kv_acc[here, width:].astype(BF16).astype(F32))
            added_ref[here] = (values * wide_ref[here, :width]).astype(BF16)

        row, column = iota((HEAD, width), 0), iota((HEAD, width), 1) % HEAD
        for n in range(count):
            here = pl.ds(n * HEAD, HEAD)
            low = low_ref[here]
            gram = dot(low, block_diagonal(low, mask), (1, 1))
            gap = wide_ref[here, width : 2 * width] - chunk_row(total, n, heads)
            lower = wide_ref[here, :width] * gram * jnp.exp(jnp.minimum(gap, 0.0))
            lower = jnp.where(row > column, lower, 0.0)
            lower_ref[here] = lower.astype(BF16)
            inverse_ref[here] = small_inverse(lower)
        size = BASE
        while size < HEAD:
            level = (row // (2 * size) == column // (2 * size)) & (row // size > column // size)
            level = jnp.where(level, 1.0, 0.0).astype(BF16)
            for n in range(count):
                here = pl.ds(n * HEAD, HEAD)
                rounded = inverse_ref[here].astype(BF16)
                inner_ref[here] = dot(lower_ref[here] * level, block_diagonal(rounded, mask)).astype(BF16)
            for n in range(count):
                here = pl.ds(n * HEAD, HEAD)
                inverse = inverse_ref[here]
                inverse_ref[here] = inverse - dot(inverse.astype(BF16), block_diagonal(inner_ref[here], mask))
            size *= 2
        for n in range(count):
            here = pl.ds(n * HEAD, HEAD)
            turned = k_ref[here].T
            turned = jnp.concatenate([turned[HEAD * h : HEAD * (h + 1)] for h in range(heads)], axis=1)
            turned = (turned * chunk_row(carry, n, heads)).astype(BF16)
            inner_ref[here] = dot(turned, block_diagonal(inverse_ref[here].astype(BF16), mask)).astype(BF16)
        for n in range(count):
            here = pl.ds(n * HEAD, HEAD)
            closing = inner_ref[here]
            removal = dot(closing, block_diagonal(taken_ref[here], mask))
            k_ref[here] = removal + jnp.where(row == column, chunk_row(dropped, n, heads), 0.0)
            inverse_ref[here] = dot(closing, block_diagonal(added_ref[here], mask))
        span = length // HEAD
        reach = 1
        while reach < span:
            for s in range(seqs):
                for n in range(s * span, (s + 1) * span, 2 * reach):
                    low, high = pl.ds(n * HEAD, HEAD), pl.ds((n + reach) * HEAD, HEAD)
                    k_ref[low], inverse_ref[low] = after(
                        (k_ref[high], inverse_ref[high]), (k_ref[low], inverse_ref[low]), mask
                    )
            reach *= 2

        lane = iota((HEAD // 2, 128), 1)
        quarter_lane = iota((HEAD // 4, 128), 1)
        for s in range(seqs):
            here = pl.ds(s * length, HEAD)
            for pair in range(heads // 2):
                r = k_ref[here, 128 * pair : 128 * (pair + 1)]
                o = inverse_ref[here, 128 * pair : 128 * (pair + 1)]
                top, bottom = r[: HEAD // 2], r[HEAD // 2 :]
                even = jnp.where(lane < HEAD, top, lanes_turned(bottom, HEAD))
                odd = jnp.where(lane < HEAD, lanes_turned(top, HEAD), bottom)
                for d in range(4):
                    dest = (s * heads + 2 * pair) * 2 + d
                    out_ref[dest, : HEAD // 2] = even if d < 2 else odd
                    packed = jnp.zeros((HEAD // 4, 128), F32)
                    for q in range(4):
                        piece = o[HEAD // 4 * q : HEAD // 4 * (q + 1)]
                        packed = jnp.where(quarter_lane // 32 == q, lanes_turned(piece, 32 * (q - d)), packed)
                    out_ref[dest, HEAD // 2 :] = packed


def owner_kernel(sources, q_ref, in_ref, out_ref, state_ref):
    lane = iota((HEAD, 128), 1)
    parts = []
    for i in range(sources):
        r, o = in_ref[i, : HEAD // 2], in_ref[i, HEAD // 2 :]
        left = jnp.concatenate([r, lanes_turned(r, HEAD)], axis=0)
        right = jnp.concatenate([lanes_turned(o, HEAD - 32 * q) for q in range(4)], axis=0)
        parts.append(jnp.where(lane < HEAD, left, jnp.where(lane < HEAD + 32, right, 0.0)))

    def combine(later, earlier):
        high, low = pieces_of(jnp.where(lane < HEAD, later, 0.0), 2)
        first_high, first_low = pieces_of(earlier, 2)
        left = jnp.concatenate([high + lanes_turned(low, HEAD), high], axis=1).astype(BF16)
        right = jnp.concatenate([first_high, first_high, first_low, first_low], axis=0).astype(BF16)
        return earlier + later - dot(left, right)

    final = composed(parts, combine)
    state_ref[...] = lanes_turned(final, HEAD)
    lane16 = iota((HEAD // 4, 128), 1)
    rows = jnp.zeros((HEAD // 4, 128), F32)
    for a in range(4):
        piece = state_ref[pl.ds(a, HEAD // 4, stride=4), :]
        rows = jnp.where(lane16 // 32 == a, lanes_turned(piece, 32 * a), rows)
    out_ref[:, :128] = rows
    state = state_ref[...]
    q = q_ref[...].astype(BF16)
    read = jnp.zeros((8, 128), F32)
    for _ in range(3):
        piece = state.astype(BF16)
        read = read + dot(q, piece)
        state = state - piece.astype(F32)
    out_ref[:, 128:] = jnp.broadcast_to(read[:1], (HEAD // 4, 128))


def body(
    layer_feed,
    address_mapping,
    content_mapping,
    beta_mapping_matrix,
    forgetting_mapping,
    logged_fading_speed,
    extra_forgetting,
    opening_probe,
):
    seqs, length, depth = layer_feed.shape
    width = address_mapping.shape[1]
    heads = width // HEAD
    all_heads = beta_mapping_matrix.shape[1]
    tokens = seqs * length
    ways = lax.axis_size("sp")
    steps = 4
    deep = depth // steps
    place = lax.axis_index("tp").astype(jnp.int32).reshape(1)
    share = (ways, 3 * HEAD // 4, 128)
    maps = pl.pallas_call(
        functools.partial(local_kernel, heads),
        grid=(steps,),
        out_shape=jax.ShapeDtypeStruct(share, F32),
        in_specs=[
            pl.BlockSpec(memory_space=pltpu.SMEM),
            pl.BlockSpec(memory_space=pltpu.SMEM),
            pl.BlockSpec((seqs, length, deep), lambda i: (0, 0, i)),
            pl.BlockSpec((deep, width), lambda i: (i, 0)),
            pl.BlockSpec((deep, width), lambda i: (i, 0)),
            pl.BlockSpec((all_heads, deep), lambda i: (0, i)),
            pl.BlockSpec((all_heads, deep), lambda i: (0, i)),
            pl.BlockSpec((seqs, heads, length), lambda i: (0, 0, 0)),
        ],
        out_specs=pl.BlockSpec(share, lambda i: (0, 0, 0)),
        scratch_shapes=[
            pltpu.VMEM((tokens, 2 * width), F32),
            pltpu.VMEM((2 * all_heads, tokens), F32),
            pltpu.VMEM((tokens, 3 * width), F32),
            pltpu.VMEM((tokens, width), F32),
            pltpu.VMEM((tokens, width), BF16),
            pltpu.VMEM((tokens, width), BF16),
            pltpu.VMEM((tokens, width), BF16),
            pltpu.VMEM((tokens, width), BF16),
            pltpu.VMEM((tokens, width), F32),
            pltpu.VMEM((tokens, width), BF16),
        ],
        compiler_params=pltpu.CompilerParams(vmem_limit_bytes=63 << 20),
        name="local_maps",
    )(
        place,
        logged_fading_speed,
        layer_feed,
        address_mapping,
        content_mapping,
        beta_mapping_matrix.T,
        forgetting_mapping.T,
        extra_forgetting.transpose(0, 2, 1),
    )
    got = lax.all_to_all(maps, "sp", 0, 0, tiled=True)
    group = lax.axis_index("sp") // 2
    query = lax.dynamic_slice_in_dim(opening_probe.reshape(seqs * heads, HEAD), group, 1, 0).astype(F32)
    query = jnp.broadcast_to(query, (8, HEAD))
    shares = pl.pallas_call(
        functools.partial(owner_kernel, ways),
        out_shape=jax.ShapeDtypeStruct((ways, 256), F32),
        scratch_shapes=[pltpu.VMEM((HEAD, 128), F32)],
        name="owner_state",
    )(query, got)
    mine = lax.all_to_all(shares.reshape(ways, 1, 256), "sp", 0, 0, tiled=True).reshape(ways, 256)
    rows = mine[:, :128].reshape(seqs * heads, 2, 4, 32).transpose(0, 2, 1, 3)
    context_memory_tensor = rows.reshape(seqs, heads, 4, HEAD).astype(BF16)
    read = mine[:, 128:160].reshape(seqs, heads, HEAD)
    read = read * lax.rsqrt(jnp.mean(read * read, axis=-1, keepdims=True) + 1e-06)
    return context_memory_tensor, read.reshape(seqs, width).astype(BF16)


def solution(mesh):
    in_specs = (
        P("grp", "sp", None),
        P(None, "tp"),
        P(None, "tp"),
        P(),
        P(),
        P("tp"),
        P("grp", "sp", "tp"),
        P("grp", "tp"),
    )
    out_specs = (P("grp", "tp", "sp", None), P("grp", "tp"))
    return jax.shard_map(body, mesh=mesh, in_specs=in_specs, out_specs=out_specs, check_vma=False)
```

time: 118 us -> 89.9 us (0.76)
  Pallas kernels: 42 us -> 19.7 us
  local copies, waits for them, and re-layouts: 8.03 us -> 2.69 us
    pallas_call x1, Pallas kernels: 39.3 us -> 16.9 us  [body(): pl.pallas_call(functools.partial(local_kernel, heads), grid=(steps,), out...]
    unnamed x12 -> x5, local copies, waits for them, and re-layouts: 5.49 us -> 0.15 us
where the time goes in v2:
time: 89.9 us; the launch traced here: 89.6 us
  starting transfers between devices  24 us (27%)
  waiting for transfers between devices  23.6 us (26%)
  Pallas kernels  19.7 us (22%)
  blocking collectives  18.2 us (20%)
  local copies, waits for them, and re-layouts  2.69 us (3%)
    all_to_all x1, starting transfers between devices, body(): got = lax.all_to_all(maps, 'sp', 0, 0, tiled=True)  24 us
    all_to_all x1, waiting for transfers between devices, body(): got = lax.all_to_all(maps, 'sp', 0, 0, tiled=True)  23.6 us
    all_to_all x1, blocking collectives, body(): lax.all_to_all(shares.reshape(ways, 1, 256), 'sp', 0, 0, tiled=True)  18.2 us
    pallas_call x1, Pallas kernels, body(): pl.pallas_call(functools.partial(local_kernel, heads), grid=(steps,), out...  16.9 us
    pallas_call x1, Pallas kernels, body(): pl.pallas_call(functools.partial(owner_kernel, ways), out_shape=jax.Shape...  2.76 us
  transfers between devices with their start and end apart: 1, of which 1 were waited for; matrix products, arithmetic and copies ran while one was open for 0% of the time, Pallas kernels for 0%

profile of v2, /device:TPU:46, one launch (start us, length us, event | category | flops | bytes accessed | tf_op | source)
XLA Modules:
  0.0 89.6 jit_solution(11076261176698112757)
XLA Ops:
  0.6 0.0 copy-start.1
  0.6 16.9 %local_maps.1 = f32[16,48,128]{2,1,0:T(8,128)} custom-call(s32[1]{0:T(128)} %bitcast.1.place_ref, f32[4]{0:T(128)} %speed_ref.1, bf16[2,512,4096]{2,1,0:T(8,128)(2,1)} %x_ref.1, bf16[4096,256]{1,0:T(8,128)(2,1)} %wk_ref.1, bf16[4096,256]{1,0:T(8,128)(2,1)} %wv_ref.1, bf16[32,4096]{1,0:T(8,128)(2,1)} %bitcast.12, bf16[32,4096]{1,0:T(8,128)(2,1)} %bitcast.13, ...), custom_call_target="tpu_custom_call" | custom-call | tf_op jit(solution)/shard_map/local_maps/pallas_call | solution.py:293
  17.6 24.0 %all-to-all-start = ((f32[16,48,128]{2,1,0:T(8,128)}), f32[16,48,128]{2,1,0:T(8,128)S(1)}, u32[]{:S(2)}, u32[]{:S(2)}) async-start(f32[16,48,128]{2,1,0:T(8,128)} %local_maps.1), calls=%async_computation | async-start | bytes 786432 | tf_op jit(solution)/shard_map/all_to_all | solution.py:332
  41.6 0.0 copy-done.1
  41.6 0.1 reshape.35
  41.7 23.6 %all-to-all-done.in_ref = f32[16,48,128]{2,1,0:T(8,128)S(1)} async-done(((f32[16,48,128]{2,1,0:T(8,128)}), f32[16,48,128]{2,1,0:T(8,128)S(1)}, u32[]{:S(2)}, u32[]{:S(2)}) %all-to-all-start) | async-done | bytes 393248 | tf_op jit(solution)/shard_map/all_to_all | solution.py:332
  65.3 0.0 copy-start
  65.3 0.6 broadcast_in_dim.13.q_ref
  65.9 0.1 copy-done
  66.0 2.8 %owner_state.1 = f32[16,256]{1,0:T(8,128)} custom-call(f32[8,64]{1,0:T(8,128)} %broadcast_in_dim.13.q_ref, f32[16,48,128]{2,1,0:T(8,128)} %copy-done), custom_call_target="tpu_custom_call" | custom-call | tf_op jit(solution)/shard_map/owner_state/pallas_call | solution.py:336
  68.8 0.7 copy.11
  69.5 18.2 %all_to_all.10 = f32[16,1,256]{2,1,0:T(1,128)S(1)} all-to-all(f32[16,1,256]{2,1,0:T(1,128)S(1)} %copy.11), channel_id=1, replica_groups=mesh['grp'=2,'sp'=16,'tp'=8] {'sp'}, dimensions={0} | all-to-all | bytes 32768 | tf_op jit(solution)/shard_map/all_to_all | solution.py:342
  87.8 0.1 mul.18
  87.9 0.1 reduce_sum.9
  88.0 0.1 reshape.39
  88.0 0.1 mul.19
  88.1 0.1 mul.20
  88.2 0.1 convert_element_type.14
  88.3 0.7 convert_element_type.16
  89.0 0.6 multiply_convert_fusion
  (6 shorter events, 0.0 us)
Async XLA Ops:
  0.6 40.9 %copy-start.1 = (bf16[2,256]{1,0:T(2,128)(2,1)S(1)}, bf16[2,256]{1,0:T(2,128)(2,1)}, u32[]{:S(2)}) copy-start(bf16[2,256]{1,0:T(2,128)(2,1)} %param.15) | copy-start | bytes 3076
  17.6 47.7 %all-to-all-start = ((f32[16,48,128]{2,1,0:T(8,128)}), f32[16,48,128]{2,1,0:T(8,128)S(1)}, u32[]{:S(2)}, u32[]{:S(2)}) async-start(f32[16,48,128]{2,1,0:T(8,128)} %local_maps.1), calls=%async_computation | async-start | bytes 786432 | tf_op jit(solution)/shard_map/all_to_all | solution.py:332
  65.3 0.8 copy-start

commit v3 on v2

v3 whole, which is shorter than its diff:
```python
import functools

import jax
import jax.numpy as jnp
from jax import lax
from jax.experimental import pallas as pl
from jax.experimental.pallas import tpu as pltpu
from jax.sharding import PartitionSpec as P

HEAD = 64
BASE = 8
F32 = jnp.float32
BF16 = jnp.bfloat16


def iota(shape, dim):
    return lax.broadcasted_iota(jnp.int32, shape, dim)


def silu(v):
    return v / (1.0 + jnp.exp(-v))


def dot(a, b, dims=(1, 0)):
    return lax.dot_general(a, b, (((dims[0],), (dims[1],)), ((), ())), preferred_element_type=F32)


def lanes_turned(x, amount):
    amount %= x.shape[1]
    return pltpu.roll(x, amount, 1) if amount else x


def split(x):
    high = x.astype(BF16)
    return high, (x - high.astype(F32)).astype(BF16)


def block_diagonal(x, lane_masks):
    heads = x.shape[1] // HEAD
    empty = jnp.zeros((x.shape[0], 128), x.dtype)
    rows = []
    for h in range(heads):
        pair = h // 2
        own = x[:, 128 * pair : 128 * (pair + 1)] * lane_masks[h % 2]
        rows.append(jnp.concatenate([own if p == pair else empty for p in range(heads // 2)], axis=1))
    return jnp.concatenate(rows, axis=0)


def pair_diagonal(x, lane_masks):
    tiles = [x[:, f : f + 128] for f in range(0, x.shape[1], 128)]
    return jnp.concatenate(
        [jnp.concatenate([t * lane_masks[h] for t in tiles], axis=1) for h in range(2)], axis=0
    )


def chunk_row(x, n, heads):
    here = x[:, 128 * (n // 2) : 128 * (n // 2 + 1)]
    turned = lanes_turned(here, HEAD)
    left, right = (here, turned) if n % 2 == 0 else (turned, here)
    first = iota((1, 128), 1) < HEAD
    return jnp.concatenate(
        [jnp.where(first, left[h : h + 1], right[h + 1 : h + 2]) for h in range(0, heads, 2)], axis=1
    )


def left_after(x):
    size = x.shape[1]
    place = iota(x.shape, 1)
    x = jnp.where(place < size - 1, lanes_turned(x, -1), 0.0)
    step = 1
    while step < size:
        x = x + jnp.where(place < size - step, lanes_turned(x, -step), 0.0)
        step *= 2
    return x


def diagonal_blocks(x):
    block = iota((BASE, x.shape[1]), 1) % HEAD // BASE
    blocks = x[:BASE]
    for r in range(1, HEAD // BASE):
        blocks = jnp.where(block == r, x[BASE * r : BASE * (r + 1)], blocks)
    return blocks


def composed(parts, combine):
    while len(parts) > 1:
        joined = [combine(parts[i + 1], parts[i]) for i in range(0, len(parts) - 1, 2)]
        parts = joined + parts[len(joined) * 2 :]
    return parts[0]


def local_kernel(
    heads, place_ref, speed_ref, x_ref, wk_ref, wv_ref, wb_ref, wf_ref, extra_ref, out_ref,
    kv_acc, small_acc, wide_ref, turned_ref, key_ref, lower_ref, inverse_ref, inner_ref, map_ref,
    blocks_ref, factor_ref
):
    step = pl.program_id(0)
    width = heads * HEAD
    seqs, length, deep = x_ref.shape
    tokens = seqs * length
    all_heads = wb_ref.shape[0]

    @pl.when(step == 0)
    def _():
        kv_acc[...] = jnp.zeros_like(kv_acc)
        small_acc[...] = jnp.zeros_like(small_acc)

    x = x_ref[...].reshape(tokens, deep)
    kv_acc[:, :width] += dot(x, wk_ref[...])
    kv_acc[:, width:] += dot(x, wv_ref[...])
    small_acc[...] += dot(jnp.concatenate([wb_ref[...], wf_ref[...]], axis=0), x, (1, 1))

    @pl.when(step == pl.num_programs(0) - 1)
    def _():
        first = place_ref[0] * heads
        half = 2 * heads
        head_of_row = iota((half, 2 * all_heads), 0) % heads
        column = iota((half, 2 * all_heads), 1)
        small = small_acc[...].astype(BF16)
        beta_pre = dot(jnp.where(column == first + head_of_row, 1.0, 0.0).astype(BF16), small)
        decay_pre = dot(jnp.where(column == all_heads + first + head_of_row, 1.0, 0.0).astype(BF16), small)
        twice = jnp.where(iota((half, heads), 0) % heads == iota((half, heads), 1), 1.0, 0.0).astype(BF16)
        row_head = iota((half, 1), 0) % heads
        speed = jnp.zeros((half, 1), F32)
        for h in range(heads):
            speed = jnp.where(row_head == h, speed_ref[h], speed)
        rate = jnp.exp(speed)
        soft = jnp.maximum(decay_pre, 0.0) + jnp.log1p(jnp.exp(-jnp.abs(decay_pre)))
        beta = 1.0 / (1.0 + jnp.exp(-beta_pre))
        decays, kept = [], []
        for s in range(seqs):
            gamma = dot(twice, extra_ref[s]) - rate * soft[:, s * length : (s + 1) * length]
            behind = left_after(gamma)
            decays.append(jnp.exp(behind))
            kept.append(jnp.exp(gamma[:, :1] + behind[:, :1]))
        stack = jnp.concatenate([p.astype(F32) for p in split(jnp.concatenate(decays, axis=1))], axis=0)
        pick = iota((2 * half, width), 0) % half == iota((2 * half, width), 1) // HEAD
        wide_ref[...] = dot(stack.T.astype(BF16), jnp.where(pick, 1.0, 0.0).astype(BF16))

        low_lanes = iota((HEAD, 128), 1) < HEAD
        lane_masks = [jnp.where(low_lanes, 1.0, 0.0).astype(BF16), jnp.where(low_lanes, 0.0, 1.0).astype(BF16)]
        same_head = iota((width, width), 0) // HEAD == iota((width, width), 1) // HEAD
        ones = jnp.where(same_head, 1.0, 0.0).astype(BF16)
        count = tokens // HEAD
        span = length // HEAD
        chunks = [pl.ds(n * HEAD, HEAD) for n in range(count)]
        for n in range(0, count, 2):
            here = pl.ds(n * HEAD, 2 * HEAD)
            keys = silu(kv_acc[here, :width].astype(BF16).astype(F32))
            norm = dot((keys * keys).astype(BF16), ones)
            keys = keys * lax.rsqrt(norm + 1e-06)
            key_ref[here] = keys.astype(BF16)
            turned = keys.astype(BF16).T
            for c in range(2):
                turned_ref[chunks[n + c]] = jnp.concatenate(
                    [turned[HEAD * h : HEAD * (h + 1), HEAD * c : HEAD * (c + 1)] for h in range(heads)], axis=1
                )
        row, column = iota((HEAD, width), 0), iota((HEAD, width), 1) % HEAD
        for n, here in enumerate(chunks):
            lower = dot(key_ref[here], block_diagonal(turned_ref[here], lane_masks))
            lower = jnp.where(row > column, lower * chunk_row(beta, n, heads), 0.0)
            lower_ref[here] = lower.astype(BF16)
            blocks = diagonal_blocks(lower)
            for f in range(0, width, 128):
                blocks_ref[pl.ds((n * width + f) // 128 * BASE, BASE)] = blocks[:, f : f + 128]
        spread_row, spread_col = iota((128, 128), 0), iota((128, 128), 1)
        spread = jnp.concatenate(
            [
                jnp.where(spread_row == spread_col // BASE * BASE + m, 1.0, 0.0).astype(BF16)
                for m in range(BASE - 1)
            ],
            axis=1,
        )
        factor_ref[...] = dot(blocks_ref[...].astype(BF16), spread)
        sets = blocks_ref.shape[0] // BASE
        solved = jnp.where(iota((BASE, 128), 0) == iota((BASE, 128), 1) % BASE, 1.0, 0.0)
        solved = jnp.broadcast_to(solved[None], (sets, BASE, 128))
        for m in range(BASE - 1):
            factor = factor_ref[:, 128 * m : 128 * (m + 1)].reshape(sets, BASE, 128)
            solved = solved - factor * solved[:, m : m + 1]
        blocks_ref[...] = solved.reshape(sets * BASE, 128)
        block = iota((BASE, width), 1) % HEAD // BASE
        for n, here in enumerate(chunks):
            own = jnp.concatenate(
                [blocks_ref[pl.ds((n * width + f) // 128 * BASE, BASE)] for f in range(0, width, 128)], axis=1
            )
            inverse_ref[here] = jnp.concatenate(
                [jnp.where(block == r, own, 0.0) for r in range(HEAD // BASE)], axis=0
            )
        level = (row // (2 * BASE) == column // (2 * BASE)) & (row // BASE > column // BASE)
        level = jnp.where(level, 1.0, 0.0).astype(BF16)
        for here in chunks:
            rounded = block_diagonal(inverse_ref[here].astype(BF16), lane_masks)
            inner_ref[here] = dot(lower_ref[here] * level, rounded).astype(BF16)
        for here in chunks:
            inverse = inverse_ref[here]
            inner = block_diagonal(inner_ref[here], lane_masks)
            inverse_ref[here] = inverse - dot(inverse.astype(BF16), inner)
        size = 2 * BASE
        while size < HEAD:
            odd = range(size, HEAD, 2 * size)
            block = iota((size, width), 1) % HEAD // size
            gap = jnp.zeros((size, width), BF16)
            for n in range(count):
                rounded = block_diagonal(inverse_ref[chunks[n]].astype(BF16), lane_masks)
                off = [
                    jnp.where(block == r // size - 1, lower_ref[pl.ds(n * HEAD + r, size)], gap) for r in odd
                ]
                inner_ref[pl.ds(n * HEAD, HEAD // 2)] = dot(jnp.concatenate(off, axis=0), rounded).astype(BF16)
            for n in range(count):
                inner = []
                for i, r in enumerate(odd):
                    inner += [gap, inner_ref[pl.ds(n * HEAD + i * size, size)]]
                inner = block_diagonal(jnp.concatenate(inner, axis=0), lane_masks)
                places = [pl.ds(n * HEAD + r, size) for r in odd]
                inverse = jnp.concatenate([inverse_ref[p] for p in places], axis=0)
                inverse = inverse - dot(inverse.astype(BF16), inner)
                for i, p in enumerate(places):
                    inverse_ref[p] = inverse[i * size : (i + 1) * size]
            size *= 2
        for n, here in enumerate(chunks):
            inverse = block_diagonal(inverse_ref[here].astype(BF16), lane_masks)
            turned = (turned_ref[here].astype(F32) * chunk_row(beta, n, heads)).astype(BF16)
            inner_ref[here] = dot(turned, inverse).astype(BF16)
        for here in chunks:
            added = (silu(kv_acc[here, width:].astype(BF16).astype(F32)) * wide_ref[here]).astype(BF16)
            for f in range(0, width, 128):
                both = jnp.concatenate([key_ref[here, f : f + 128], added[:, f : f + 128]], axis=1)
                map_ref[here, 2 * f : 2 * f + 256] = dot(inner_ref[here, f : f + 128], pair_diagonal(both, lane_masks))
        reach = 1
        while reach < span:
            for n in range(0, count, 2 * reach):
                early, late = chunks[n], chunks[n + reach]
                for f in range(0, 2 * width, 256):
                    before, later = map_ref[early, f : f + 256], map_ref[late, f : f + 256]
                    carried = dot(later[:, :128].astype(BF16), pair_diagonal(before.astype(BF16), lane_masks))
                    map_ref[early, f : f + 256] = before + later - carried
            reach *= 2

        lane = iota((HEAD // 2, 128), 1)
        quarter_lane = iota((HEAD // 4, 128), 1)
        lane_head = iota((1, width), 1) // HEAD
        for s in range(seqs):
            here = chunks[s * span]
            keep = jnp.zeros((1, width), F32)
            for h in range(heads):
                keep = jnp.where(lane_head == h, kept[s][h : h + 1], keep)
            for pair in range(heads // 2):
                part = slice(128 * pair, 128 * (pair + 1))
                r = keep[:, part] * map_ref[here, 256 * pair : 256 * pair + 128]
                r = r + jnp.where(row[:, part] == column[:, part], 1.0 - keep[:, part], 0.0)
                o = map_ref[here, 256 * pair + 128 : 256 * (pair + 1)]
                top, bottom = r[: HEAD // 2], r[HEAD // 2 :]
                even = jnp.where(lane < HEAD, top, lanes_turned(bottom, HEAD))
                odd = jnp.where(lane < HEAD, lanes_turned(top, HEAD), bottom)
                for d in range(4):
                    dest = (s * heads + 2 * pair) * 2 + d
                    out_ref[dest, : HEAD // 2] = even if d < 2 else odd
                    packed = jnp.zeros((HEAD // 4, 128), F32)
                    for q in range(4):
                        piece = o[HEAD // 4 * q : HEAD // 4 * (q + 1)]
                        packed = jnp.where(quarter_lane // 32 == q, lanes_turned(piece, 32 * (q - d)), packed)
                    out_ref[dest, HEAD // 2 :] = packed


def owner_kernel(heads, place_ref, probe_ref, in_ref, out_ref):
    sources = in_ref.shape[0]
    lane = iota((HEAD, 128), 1)
    parts = []
    for i in range(sources):
        r, o = in_ref[i, : HEAD // 2], in_ref[i, HEAD // 2 :]
        left = jnp.concatenate([r, lanes_turned(r, HEAD)], axis=0)
        right = jnp.concatenate([lanes_turned(o, HEAD - 32 * q) for q in range(4)], axis=0)
        parts.append(jnp.where(lane < HEAD, left, jnp.where(lane < HEAD + 32, right, 0.0)))

    def combine(later, earlier):
        removal = jnp.where(lane < HEAD, later, 0.0)
        high = removal.astype(BF16)
        low = lanes_turned(removal - high.astype(F32), HEAD).astype(BF16)
        first_high, first_low = split(earlier)
        left = jnp.concatenate([high + low, high], axis=1)
        right = jnp.concatenate([first_high, first_high, first_low, first_low], axis=0)
        return earlier + later - dot(left, right)

    state = lanes_turned(composed(parts, combine), HEAD)
    share = HEAD // sources
    for j in range(sources):
        out_ref[j, :share] = state[share * j : share * (j + 1)]
    group = place_ref[0] // 2
    probe = probe_ref[...].astype(F32)
    probe = jnp.where(iota(probe.shape, 0) == group // heads, probe, 0.0)
    probe = jnp.sum(probe, axis=0, keepdims=True)
    query = jnp.zeros((1, 128), F32)
    for h in range(heads):
        pair = probe[:, 128 * (h // 2) : 128 * (h // 2 + 1)]
        query = jnp.where(group % heads == h, lanes_turned(pair, HEAD) if h % 2 else pair, query)
    query = jnp.broadcast_to(query[:, :HEAD], (8, HEAD)).astype(BF16)
    read = jnp.zeros((8, 128), F32)
    for _ in range(3):
        piece = state.astype(BF16)
        read = read + dot(query, piece)
        state = state - piece.astype(F32)
    for j in range(sources):
        out_ref[j, share:] = read[share:]


def result_kernel(in_ref, rows_ref, read_ref):
    seqs, heads, share, _ = rows_ref.shape
    lane = iota((8, 128), 1)
    reads = []
    for g in range(seqs * heads):
        both = jnp.where(lane < HEAD // 2, in_ref[2 * g], lanes_turned(in_ref[2 * g + 1], HEAD // 2))
        rows_ref[g // heads, g % heads] = both[:share, :HEAD].astype(BF16)
        read = jnp.where(lane < HEAD, both, 0.0)[share : share + 1]
        mean = jnp.sum(read * read, axis=1, keepdims=True) / HEAD
        reads.append(read * lax.rsqrt(mean + 1e-06))
    for s in range(seqs):
        own = reads[s * heads : (s + 1) * heads]
        pairs = [own[h] + lanes_turned(own[h + 1], HEAD) for h in range(0, heads, 2)]
        read_ref[pl.ds(s, 1)] = jnp.concatenate(pairs, axis=1).astype(BF16)


def body(
    layer_feed,
    address_mapping,
    content_mapping,
    beta_mapping_matrix,
    forgetting_mapping,
    logged_fading_speed,
    extra_forgetting,
    opening_probe,
):
    seqs, length, depth = layer_feed.shape
    width = address_mapping.shape[1]
    heads = width // HEAD
    all_heads = beta_mapping_matrix.shape[1]
    tokens = seqs * length
    ways = lax.axis_size("sp")
    steps = 4
    deep = depth // steps
    place = lax.axis_index("tp").astype(jnp.int32).reshape(1)
    share = (ways, 3 * HEAD // 4, 128)
    maps = pl.pallas_call(
        functools.partial(local_kernel, heads),
        grid=(steps,),
        out_shape=jax.ShapeDtypeStruct(share, F32),
        in_specs=[
            pl.BlockSpec(memory_space=pltpu.SMEM),
            pl.BlockSpec(memory_space=pltpu.SMEM),
            pl.BlockSpec((seqs, length, deep), lambda i: (0, 0, i)),
            pl.BlockSpec((deep, width), lambda i: (i, 0)),
            pl.BlockSpec((deep, width), lambda i: (i, 0)),
            pl.BlockSpec((all_heads, deep), lambda i: (0, i)),
            pl.BlockSpec((all_heads, deep), lambda i: (0, i)),
            pl.BlockSpec((seqs, heads, length), lambda i: (0, 0, 0)),
        ],
        out_specs=pl.BlockSpec(share, lambda i: (0, 0, 0)),
        scratch_shapes=[
            pltpu.VMEM((tokens, 2 * width), F32),
            pltpu.VMEM((2 * all_heads, tokens), F32),
            pltpu.VMEM((tokens, width), F32),
            pltpu.VMEM((tokens, width), BF16),
            pltpu.VMEM((tokens, width), BF16),
            pltpu.VMEM((tokens, width), BF16),
            pltpu.VMEM((tokens, width), F32),
            pltpu.VMEM((tokens, width), BF16),
            pltpu.VMEM((tokens, 2 * width), F32),
            pltpu.VMEM((tokens * width // HEAD // 128 * BASE, 128), F32),
            pltpu.VMEM((tokens * width // HEAD // 128 * BASE, 128 * (BASE - 1)), F32),
        ],
        compiler_params=pltpu.CompilerParams(vmem_limit_bytes=63 << 20),
        name="local_maps",
    )(
        place,
        logged_fading_speed,
        layer_feed,
        address_mapping,
        content_mapping,
        beta_mapping_matrix.T,
        forgetting_mapping.T,
        extra_forgetting.transpose(0, 2, 1),
    )
    got = lax.all_to_all(maps, "sp", 0, 0, tiled=True)
    turn = lax.axis_index("sp").astype(jnp.int32).reshape(1)
    shares = pl.pallas_call(
        functools.partial(owner_kernel, heads),
        out_shape=jax.ShapeDtypeStruct((ways, 8, 128), F32),
        in_specs=[
            pl.BlockSpec(memory_space=pltpu.SMEM),
            pl.BlockSpec(memory_space=pltpu.VMEM),
            pl.BlockSpec(memory_space=pltpu.VMEM),
        ],
        compiler_params=pltpu.CompilerParams(vmem_limit_bytes=8 << 20),
        name="owner_state",
    )(turn, opening_probe, got)
    mine = lax.all_to_all(shares, "sp", 0, 0, tiled=True)
    return pl.pallas_call(
        result_kernel,
        out_shape=(
            jax.ShapeDtypeStruct((seqs, heads, HEAD // ways, HEAD), BF16),
            jax.ShapeDtypeStruct((seqs, width), BF16),
        ),
        compiler_params=pltpu.CompilerParams(vmem_limit_bytes=8 << 20),
        name="results",
    )(mine)


def solution(mesh):
    in_specs = (
        P("grp", "sp", None),
        P(None, "tp"),
        P(None, "tp"),
        P(),
        P(),
        P("tp"),
        P("grp", "sp", "tp"),
        P("grp", "tp"),
    )
    out_specs = (P("grp", "tp", "sp", None), P("grp", "tp"))
    return jax.shard_map(body, mesh=mesh, in_specs=in_specs, out_specs=out_specs, check_vma=False)
```

time: 89.9 us -> 84.8 us (0.943)
  local copies, waits for them, and re-layouts: 2.69 us -> 0.01 us
  Pallas kernels: 19.7 us -> 17.6 us
    pallas_call x1, Pallas kernels: 16.9 us -> 15.7 us  [body(): pl.pallas_call(functools.partial(local_kernel, heads), grid=(steps,), out...]
    pallas_call x1 -> x2, Pallas kernels: 2.76 us -> 1.97 us  [the longest x1 1.14 us: body(): pl.pallas_call(functools.partial(owner_kernel, heads), out_shape=jax.Shap...]
where the time goes in v3:
time: 84.8 us; the launch traced here: 84.4 us
  starting transfers between devices  24 us (28%)
  waiting for transfers between devices  23.7 us (28%)
  blocking collectives  18.4 us (22%)
  Pallas kernels  17.6 us (21%)
    all_to_all x1, starting transfers between devices, body(): got = lax.all_to_all(maps, 'sp', 0, 0, tiled=True)  24 us
    all_to_all x1, waiting for transfers between devices, body(): got = lax.all_to_all(maps, 'sp', 0, 0, tiled=True)  23.7 us
    all_to_all x1, blocking collectives, body(): mine = lax.all_to_all(shares, 'sp', 0, 0, tiled=True)  18.4 us
    pallas_call x1, Pallas kernels, body(): pl.pallas_call(functools.partial(local_kernel, heads), grid=(steps,), out...  15.7 us
  transfers between devices with their start and end apart: 1, of which 1 were waited for; matrix products, arithmetic and copies ran while one was open for 0% of the time, Pallas kernels for 0%

profile of v3, /device:TPU:46, one launch (start us, length us, event | category | flops | bytes accessed | tf_op | source)
XLA Modules:
  0.0 84.4 jit_solution(10228216091507934016)
XLA Ops:
  0.6 0.0 copy-start
  0.6 15.7 %local_maps.1 = f32[16,48,128]{2,1,0:T(8,128)} custom-call(s32[1]{0:T(128)} %bitcast.1.place_ref, f32[4]{0:T(128)} %speed_ref.1, bf16[2,512,4096]{2,1,0:T(8,128)(2,1)} %x_ref.1, bf16[4096,256]{1,0:T(8,128)(2,1)} %wk_ref.1, bf16[4096,256]{1,0:T(8,128)(2,1)} %wv_ref.1, bf16[32,4096]{1,0:T(8,128)(2,1)} %bitcast.5, bf16[32,4096]{1,0:T(8,128)(2,1)} %bitcast.6, ...), custom_call_target="tpu_custom_call" | custom-call | tf_op jit(solution)/shard_map/local_maps/pallas_call | solution.py:343
  16.3 24.0 %all-to-all-start = ((f32[16,48,128]{2,1,0:T(8,128)}), f32[16,48,128]{2,1,0:T(8,128)S(1)}, u32[]{:S(2)}, u32[]{:S(2)}) async-start(f32[16,48,128]{2,1,0:T(8,128)} %local_maps.1), calls=%async_computation | async-start | bytes 786432 | tf_op jit(solution)/shard_map/all_to_all | solution.py:383
  40.3 23.7 %all-to-all-done.in_ref = f32[16,48,128]{2,1,0:T(8,128)S(1)} async-done(((f32[16,48,128]{2,1,0:T(8,128)}), f32[16,48,128]{2,1,0:T(8,128)S(1)}, u32[]{:S(2)}, u32[]{:S(2)}) %all-to-all-start) | async-done | bytes 393248 | tf_op jit(solution)/shard_map/all_to_all | solution.py:383
  64.0 0.0 copy-done
  64.0 1.1 %owner_state.1 = f32[16,8,128]{2,1,0:T(8,128)S(1)} custom-call(s32[1]{0:T(128)} %bitcast.place_ref, bf16[2,256]{1,0:T(2,128)(2,1)S(1)} %copy-done, f32[16,48,128]{2,1,0:T(8,128)S(1)} %all-to-all-done.in_ref), custom_call_target="tpu_custom_call" | custom-call | tf_op jit(solution)/shard_map/owner_state/pallas_call | solution.py:385
  65.2 18.4 %all_to_all.10.in_ref = f32[16,8,128]{2,1,0:T(8,128)S(1)} all-to-all(f32[16,8,128]{2,1,0:T(8,128)S(1)} %owner_state.1), channel_id=1, replica_groups=mesh['grp'=2,'sp'=16,'tp'=8] {'sp'}, dimensions={0} | all-to-all | bytes 131072 | tf_op jit(solution)/shard_map/all_to_all | solution.py:396
  83.6 0.8 results.1
Async XLA Ops:
  0.6 63.4 %copy-start = (bf16[2,256]{1,0:T(2,128)(2,1)S(1)}, bf16[2,256]{1,0:T(2,128)(2,1)}, u32[]{:S(2)}) copy-start(bf16[2,256]{1,0:T(2,128)(2,1)} %probe_ref.1) | copy-start | bytes 3076
  16.3 47.7 %all-to-all-start = ((f32[16,48,128]{2,1,0:T(8,128)}), f32[16,48,128]{2,1,0:T(8,128)S(1)}, u32[]{:S(2)}, u32[]{:S(2)}) async-start(f32[16,48,128]{2,1,0:T(8,128)} %local_maps.1), calls=%async_computation | async-start | bytes 786432 | tf_op jit(solution)/shard_map/all_to_all | solution.py:383

commit v4 on v3

--- a/solution.py
+++ b/solution.py
@@ -90,7 +90,7 @@
 
 
 def local_kernel(
-    heads, place_ref, speed_ref, x_ref, wk_ref, wv_ref, wb_ref, wf_ref, extra_ref, out_ref,
+    heads, place_ref, speed_ref, x_ref, wk_ref, wv_ref, wb_ref, wf_ref, extra_ref, kept_ref, sent_ref,
     kv_acc, small_acc, wide_ref, turned_ref, key_ref, lower_ref, inverse_ref, inner_ref, map_ref,
     blocks_ref, factor_ref
 ):
@@ -237,79 +237,110 @@
                     map_ref[early, f : f + 256] = before + later - carried
             reach *= 2
 
-        lane = iota((HEAD // 2, 128), 1)
-        quarter_lane = iota((HEAD // 4, 128), 1)
         lane_head = iota((1, width), 1) // HEAD
+        maps = []
         for s in range(seqs):
             here = chunks[s * span]
             keep = jnp.zeros((1, width), F32)
             for h in range(heads):
                 keep = jnp.where(lane_head == h, kept[s][h : h + 1], keep)
-            for pair in range(heads // 2):
-                part = slice(128 * pair, 128 * (pair + 1))
-                r = keep[:, part] * map_ref[here, 256 * pair : 256 * pair + 128]
-                r = r + jnp.where(row[:, part] == column[:, part], 1.0 - keep[:, part], 0.0)
-                o = map_ref[here, 256 * pair + 128 : 256 * (pair + 1)]
-                top, bottom = r[: HEAD // 2], r[HEAD // 2 :]
-                even = jnp.where(lane < HEAD, top, lanes_turned(bottom, HEAD))
-                odd = jnp.where(lane < HEAD, lanes_turned(top, HEAD), bottom)
-                for d in range(4):
-                    dest = (s * heads + 2 * pair) * 2 + d
-                    out_ref[dest, : HEAD // 2] = even if d < 2 else odd
-                    packed = jnp.zeros((HEAD // 4, 128), F32)
-                    for q in range(4):
-                        piece = o[HEAD // 4 * q : HEAD // 4 * (q + 1)]
-                        packed = jnp.where(quarter_lane // 32 == q, lanes_turned(piece, 32 * (q - d)), packed)
-                    out_ref[dest, HEAD // 2 :] = packed
-
-
-def owner_kernel(heads, place_ref, probe_ref, in_ref, out_ref):
-    sources = in_ref.shape[0]
-    lane = iota((HEAD, 128), 1)
-    parts = []
-    for i in range(sources):
-        r, o = in_ref[i, : HEAD // 2], in_ref[i, HEAD // 2 :]
-        left = jnp.concatenate([r, lanes_turned(r, HEAD)], axis=0)
-        right = jnp.concatenate([lanes_turned(o, HEAD - 32 * q) for q in range(4)], axis=0)
-        parts.append(jnp.where(lane < HEAD, left, jnp.where(lane < HEAD + 32, right, 0.0)))
-
-    def combine(later, earlier):
-        removal = jnp.where(lane < HEAD, later, 0.0)
-        high = removal.astype(BF16)
-        low = lanes_turned(removal - high.astype(F32), HEAD).astype(BF16)
-        first_high, first_low = split(earlier)
-        left = jnp.concatenate([high + low, high], axis=1)
-        right = jnp.concatenate([first_high, first_high, first_low, first_low], axis=0)
-        return earlier + later - dot(left, right)
-
-    state = lanes_turned(composed(parts, combine), HEAD)
-    share = HEAD // sources
-    for j in range(sources):
-        out_ref[j, :share] = state[share * j : share * (j + 1)]
-    group = place_ref[0] // 2
+            tiles = []
+            for f in range(0, width, 128):
+                part = slice(f, f + 128)
+                removal = keep[:, part] * map_ref[here, 2 * f : 2 * f + 128]
+                tiles.append(removal + jnp.where(row[:, part] == column[:, part], 1.0 - keep[:, part], 0.0))
+                tiles.append(map_ref[here, 2 * f + 128 : 2 * f + 256])
+            maps.append(jnp.concatenate(tiles, axis=1))
+        shared_out(place_ref[1] % 2, maps, kept_ref, sent_ref)
+
+
+def shared_out(bit, halves, kept_ref, sent_ref):
+    kept_ref[...] = jnp.where(bit == 0, halves[0], halves[1])
+    sent_ref[...] = jnp.where(bit == 0, halves[1], halves[0])
+
+
+def in_order(bit, own, other):
+    return jnp.where(bit == 0, other, own), jnp.where(bit == 0, own, other)
+
+
+def pair_after(later, earlier):
+    lane_masks = head_masks()
+    high, low = split(later[:, :128])
+    first_high, first_low = split(earlier)
+    product = dot(jnp.concatenate([high, low], axis=1), jnp.concatenate([pair_diagonal(first_high, lane_masks)] * 2, axis=0))
+    return earlier + later - (product + dot(high, pair_diagonal(first_low, lane_masks)))
+
+
+def widened(x):
+    x = jnp.where(iota(x.shape, 1) < HEAD, x, 0.0)
+    high = x.astype(BF16)
+    low = lanes_turned(x - high.astype(F32), HEAD).astype(BF16)
+    return jnp.concatenate([high + low, high], axis=1)
+
+
+def stacked(x):
+    high, low = split(x)
+    return jnp.concatenate([high, high, low, low], axis=0)
+
+
+def first_kernel(place_ref, own_ref, other_ref, kept_ref, sent_ref):
+    later, earlier = in_order(place_ref[0] % 2, own_ref[...], other_ref[...])
+    pairs = [pair_after(later[:, f : f + 256], earlier[:, f : f + 256]) for f in range(0, later.shape[1], 256)]
+    shared_out(place_ref[0] // 2 % 2, pairs, kept_ref, sent_ref)
+
+
+def second_kernel(place_ref, own_ref, other_ref, kept_ref, sent_ref):
+    pair = pair_after(*in_order(place_ref[0] // 2 % 2, own_ref[...], other_ref[...]))
+    removal, offset = pair[:, :128], pair[:, 128:]
+    low_lanes = iota(removal.shape, 1) < HEAD
+    even = jnp.where(low_lanes, removal, lanes_turned(offset, HEAD))
+    odd = jnp.where(low_lanes, lanes_turned(removal, HEAD), offset)
+    shared_out(place_ref[0] // 4 % 2, (even, odd), kept_ref, sent_ref)
+
+
+def third_kernel(heads, place_ref, probe_ref, own_ref, other_ref, out_ref):
+    place = place_ref[0]
+    later, earlier = in_order(place // 4 % 2, own_ref[...], other_ref[...])
+    state = earlier + later - dot(widened(later), stacked(earlier))
+    shape = state.shape
+    through = jnp.where(iota(shape, 0) == iota(shape, 1), 1.0 - state, -state)
+    through = jnp.where(iota(shape, 1) < HEAD, through, state)
     probe = probe_ref[...].astype(F32)
-    probe = jnp.where(iota(probe.shape, 0) == group // heads, probe, 0.0)
-    probe = jnp.sum(probe, axis=0, keepdims=True)
+    probe = jnp.sum(jnp.where(iota(probe.shape, 0) == place % 2, probe, 0.0), axis=0, keepdims=True)
+    head = place // 2 % 2 * 2 + place // 4 % 2
     query = jnp.zeros((1, 128), F32)
     for h in range(heads):
         pair = probe[:, 128 * (h // 2) : 128 * (h // 2 + 1)]
-        query = jnp.where(group % heads == h, lanes_turned(pair, HEAD) if h % 2 else pair, query)
+        query = jnp.where(head == h, lanes_turned(pair, HEAD) if h % 2 else pair, query)
     query = jnp.broadcast_to(query[:, :HEAD], (8, HEAD)).astype(BF16)
     read = jnp.zeros((8, 128), F32)
+    rest = through
     for _ in range(3):
-        piece = state.astype(BF16)
+        piece = rest.astype(BF16)
         read = read + dot(query, piece)
-        state = state - piece.astype(F32)
-    for j in range(sources):
-        out_ref[j, share:] = read[share:]
+        rest = rest - piece.astype(F32)
+    half = HEAD // 2
+    packed = jnp.where(iota((half, 128), 1) < HEAD, lanes_turned(state[:half], HEAD), state[half:])
+    ways = out_ref.shape[0]
+    share = HEAD // ways
+    is_late = place >= ways // 2
+    for j in range(ways):
+        rows = jnp.concatenate([through[share * j : share * (j + 1)], read[share:]], axis=0)
+        out_ref[j, :8] = jnp.where(is_late, rows, packed[:8])
+        out_ref[j, 8:] = packed[8:]
 
 
 def result_kernel(in_ref, rows_ref, read_ref):
     seqs, heads, share, _ = rows_ref.shape
+    ways = in_ref.shape[0]
     lane = iota((8, 128), 1)
     reads = []
     for g in range(seqs * heads):
-        both = jnp.where(lane < HEAD // 2, in_ref[2 * g], lanes_turned(in_ref[2 * g + 1], HEAD // 2))
+        source = g // heads + g % heads // 2 * 2 + g % 2 * 4
+        late = in_ref[source + ways // 2, :8]
+        packed = in_ref[source]
+        early = jnp.concatenate([packed, lanes_turned(packed, HEAD)], axis=0)
+        both = dot(widened(late), stacked(early)) + lanes_turned(late, HEAD)
         rows_ref[g // heads, g % heads] = both[:share, :HEAD].astype(BF16)
         read = jnp.where(lane < HEAD, both, 0.0)[share : share + 1]
         mean = jnp.sum(read * read, axis=1, keepdims=True) / HEAD
@@ -318,6 +349,11 @@
         own = reads[s * heads : (s + 1) * heads]
         pairs = [own[h] + lanes_turned(own[h + 1], HEAD) for h in range(0, heads, 2)]
         read_ref[pl.ds(s, 1)] = jnp.concatenate(pairs, axis=1).astype(BF16)
+
+
+def head_masks():
+    low_lanes = iota((HEAD, 128), 1) < HEAD
+    return [jnp.where(low_lanes, 1.0, 0.0).astype(BF16), jnp.where(low_lanes, 0.0, 1.0).astype(BF16)]
 
 
 def body(
@@ -338,12 +374,13 @@
     ways = lax.axis_size("sp")
     steps = 4
     deep = depth // steps
-    place = lax.axis_index("tp").astype(jnp.int32).reshape(1)
-    share = (ways, 3 * HEAD // 4, 128)
-    maps = pl.pallas_call(
+    turn = lax.axis_index("sp").astype(jnp.int32).reshape(1)
+    place = jnp.concatenate([lax.axis_index("tp").astype(jnp.int32).reshape(1), turn])
+    share = (HEAD, 2 * width)
+    kept, sent = pl.pallas_call(
         functools.partial(local_kernel, heads),
         grid=(steps,),
-        out_shape=jax.ShapeDtypeStruct(share, F32),
+        out_shape=(jax.ShapeDtypeStruct(share, F32),) * 2,
         in_specs=[
             pl.BlockSpec(memory_space=pltpu.SMEM),
             pl.BlockSpec(memory_space=pltpu.SMEM),
@@ -354,7 +391,7 @@
             pl.BlockSpec((all_heads, deep), lambda i: (0, i)),
             pl.BlockSpec((seqs, heads, length), lambda i: (0, 0, 0)),
         ],
-        out_specs=pl.BlockSpec(share, lambda i: (0, 0, 0)),
+        out_specs=(pl.BlockSpec(share, lambda i: (0, 0)),) * 2,
         scratch_shapes=[
             pltpu.VMEM((tokens, 2 * width), F32),
             pltpu.VMEM((2 * all_heads, tokens), F32),
@@ -380,19 +417,27 @@
         forgetting_mapping.T,
         extra_forgetting.transpose(0, 2, 1),
     )
-    got = lax.all_to_all(maps, "sp", 0, 0, tiled=True)
-    turn = lax.axis_index("sp").astype(jnp.int32).reshape(1)
+    scalar, vector = pl.BlockSpec(memory_space=pltpu.SMEM), pl.BlockSpec(memory_space=pltpu.VMEM)
+    small = pltpu.CompilerParams(vmem_limit_bytes=8 << 20)
+
+    def swapped(x, distance):
+        return lax.ppermute(x, "sp", [(i, i ^ distance) for i in range(ways)])
+
+    for kernel, distance, lanes, name in ((first_kernel, 1, width, "first"), (second_kernel, 2, width // 2, "second")):
+        kept, sent = pl.pallas_call(
+            kernel,
+            out_shape=(jax.ShapeDtypeStruct((HEAD, lanes), F32),) * 2,
+            in_specs=[scalar, vector, vector],
+            compiler_params=small,
+            name=name,
+        )(turn, kept, swapped(sent, distance))
     shares = pl.pallas_call(
-        functools.partial(owner_kernel, heads),
-        out_shape=jax.ShapeDtypeStruct((ways, 8, 128), F32),
-        in_specs=[
-            pl.BlockSpec(memory_space=pltpu.SMEM),
-            pl.BlockSpec(memory_space=pltpu.VMEM),
-            pl.BlockSpec(memory_space=pltpu.VMEM),
-        ],
-        compiler_params=pltpu.CompilerParams(vmem_limit_bytes=8 << 20),
-        name="owner_state",
-    )(turn, opening_probe, got)
+        functools.partial(third_kernel, heads),
+        out_shape=jax.ShapeDtypeStruct((ways, HEAD // 2, 128), F32),
+        in_specs=[scalar, vector, vector, vector],
+        compiler_params=small,
+        name="third",
+    )(turn, opening_probe, kept, swapped(sent, 4))
     mine = lax.all_to_all(shares, "sp", 0, 0, tiled=True)
     return pl.pallas_call(
         result_kernel,

time: 84.8 us -> 78.8 us (0.929)
  waiting for transfers between devices: 23.7 us -> 8.17 us
  blocking collectives: 18.4 us -> 32.2 us
  starting transfers between devices: 24 us -> 18.7 us
  local copies, waits for them, and re-layouts: 0.01 us -> 0.91 us
    all_to_all x1 -> x0, starting transfers between devices: 24 us -> none  [body(): got = lax.all_to_all(maps, 'sp', 0, 0, tiled=True)]
    all_to_all x1 -> x0, waiting for transfers between devices: 23.7 us -> none  [body(): got = lax.all_to_all(maps, 'sp', 0, 0, tiled=True)]
    ppermute x0 -> x3, starting transfers between devices: none -> 18.7 us  [swapped(): return lax.ppermute(x, 'sp', [(i, i ^ distance) for i in range(ways)])]
    all_to_all x1, blocking collectives: 18.4 us -> 32.2 us  [body(): mine = lax.all_to_all(shares, 'sp', 0, 0, tiled=True)]
    ppermute x0 -> x3, waiting for transfers between devices: none -> 8.17 us  [swapped(): return lax.ppermute(x, 'sp', [(i, i ^ distance) for i in range(ways)])]
    unnamed x2 -> x4, local copies, waits for them, and re-layouts: 0.01 us -> 0.91 us
  transfers between devices with their start and end apart: 1 -> 3, of which waited for: 1 -> 3; matrix products, arithmetic and copies ran while one was open for 0% -> 0% of each run, Pallas kernels for 0% -> 0%
where the time goes in v4:
time: 78.8 us; the launch traced here: 78.6 us
  blocking collectives  32.2 us (41%)
  starting transfers between devices  18.7 us (24%)
  Pallas kernels  17.3 us (22%)
  waiting for transfers between devices  8.17 us (10%)
  local copies, waits for them, and re-layouts  0.91 us (1%)
    all_to_all x1, blocking collectives, body(): mine = lax.all_to_all(shares, 'sp', 0, 0, tiled=True)  32.2 us
    ppermute x3, starting transfers between devices, swapped(): return lax.ppermute(x, 'sp', [(i, i ^ distance) for i in range(ways)])  18.7 us
    pallas_call x1, Pallas kernels, body(): pl.pallas_call(functools.partial(local_kernel, heads), grid=(steps,), out...  15.5 us
    ppermute x3, waiting for transfers between devices, swapped(): return lax.ppermute(x, 'sp', [(i, i ^ distance) for i in range(ways)])  8.17 us
  transfers between devices with their start and end apart: 3, of which 3 were waited for; matrix products, arithmetic and copies ran while one was open for 0% of the time, Pallas kernels for 0%

profile of v4, /device:TPU:46, one launch (start us, length us, event | category | flops | bytes accessed | tf_op | source)
XLA Modules:
  0.0 78.6 jit_solution(6950930363487538782)
XLA Ops:
  0.6 0.6 pad_add_fusion.place_ref
  1.3 0.0 copy-start.1
  1.3 15.5 %local_maps.1 = (f32[64,512]{1,0:T(8,128)}, f32[64,512]{1,0:T(8,128)}) custom-call(s32[2]{0:T(128)} %pad_add_fusion.place_ref, f32[4]{0:T(128)} %speed_ref.1, bf16[2,512,4096]{2,1,0:T(8,128)(2,1)} %x_ref.1, bf16[4096,256]{1,0:T(8,128)(2,1)} %wk_ref.1, bf16[4096,256]{1,0:T(8,128)(2,1)} %wv_ref.1, bf16[32,4096]{1,0:T(8,128)(2,1)} %bitcast.5, ...), custom_call_target="tpu_custom_call" | custom-call | tf_op jit(solution)/shard_map/local_maps/pallas_call | solution.py:380
  16.8 2.8 %collective-permute-start = (f32[64,512]{1,0:T(8,128)}, f32[64,512]{1,0:T(8,128)S(1)}, u32[]{:S(2)}, u32[]{:S(2)}) collective-permute-start(f32[64,512]{1,0:T(8,128)} %get-tuple-element.9), channel_id=1, source_target_pairs={{0,8},{8,0},{16,24},{24,16},{32,40},{40,32},{48,56},{56,48},{64,72... | collective-permute-start | bytes 393224 | tf_op jit(solution)/shard_map/ppermute | solution.py:424
  19.6 3.8 %collective-permute-done.other_ref = f32[64,512]{1,0:T(8,128)S(1)} collective-permute-done((f32[64,512]{1,0:T(8,128)}, f32[64,512]{1,0:T(8,128)S(1)}, u32[]{:S(2)}, u32[]{:S(2)}) %collective-permute-start) | collective-permute-done | bytes 131104 | tf_op jit(solution)/shard_map/ppermute | solution.py:424
  23.4 0.0 copy-start
  23.4 0.9 %copy-done = f32[64,512]{1,0:T(8,128)S(1)} copy-done((f32[64,512]{1,0:T(8,128)S(1)}, f32[64,512]{1,0:T(8,128)}, u32[]{:S(2)}) %copy-start) | copy-done | bytes 131096
  24.3 0.2 first.1
  24.5 5.1 %collective-permute-start.1 = (f32[64,256]{1,0:T(8,128)S(1)}, f32[64,256]{1,0:T(8,128)S(1)}, u32[]{:S(2)}, u32[]{:S(2)}) collective-permute-start(f32[64,256]{1,0:T(8,128)S(1)} %get-tuple-element.11), channel_id=1, source_target_pairs={{0,16},{8,24},{16,0},{24,8},{32,48},{40,56},{48,32},{56,40},{64,80... | collective-permute-start | bytes 196616 | tf_op jit(solution)/shard_map/ppermute | solution.py:424
  29.6 2.5 %collective-permute-done.1.other_ref = f32[64,256]{1,0:T(8,128)S(1)} collective-permute-done((f32[64,256]{1,0:T(8,128)S(1)}, f32[64,256]{1,0:T(8,128)S(1)}, u32[]{:S(2)}, u32[]{:S(2)}) %collective-permute-start.1) | collective-permute-done | bytes 65568 | tf_op jit(solution)/shard_map/ppermute | solution.py:424
  32.1 0.2 second.1
  32.4 10.8 %collective-permute-start.2 = (f32[64,128]{1,0:T(8,128)S(1)}, f32[64,128]{1,0:T(8,128)S(1)}, u32[]{:S(2)}, u32[]{:S(2)}) collective-permute-start(f32[64,128]{1,0:T(8,128)S(1)} %get-tuple-element.13), channel_id=1, source_target_pairs={{0,32},{8,40},{16,48},{24,56},{32,0},{40,8},{48,16},{56,24},{64,96... | collective-permute-start | bytes 98312 | tf_op jit(solution)/shard_map/ppermute | solution.py:424
  43.1 1.9 %collective-permute-done.2.other_ref = f32[64,128]{1,0:T(8,128)S(1)} collective-permute-done((f32[64,128]{1,0:T(8,128)S(1)}, f32[64,128]{1,0:T(8,128)S(1)}, u32[]{:S(2)}, u32[]{:S(2)}) %collective-permute-start.2) | collective-permute-done | bytes 32800 | tf_op jit(solution)/shard_map/ppermute | solution.py:424
  45.0 0.0 copy-done.1
  45.0 0.3 third.1
  45.4 32.2 %all_to_all.5.in_ref = f32[16,32,128]{2,1,0:T(8,128)S(1)} all-to-all(f32[16,32,128]{2,1,0:T(8,128)S(1)} %third.1), channel_id=1, replica_groups=mesh['grp'=2,'sp'=16,'tp'=8] {'sp'}, dimensions={0} | all-to-all | bytes 524288 | tf_op jit(solution)/shard_map/all_to_all | solution.py:441
  77.6 1.0 %results.1 = (bf16[2,4,4,64]{3,2,1,0:T(4,128)(2,1)}, bf16[2,256]{1,0:T(2,128)(2,1)}) custom-call(f32[16,32,128]{2,1,0:T(8,128)S(1)} %all_to_all.5.in_ref), custom_call_target="tpu_custom_call" | custom-call | tf_op jit(solution)/shard_map/results/pallas_call | solution.py:442
Async XLA Ops:
  1.3 43.8 %copy-start.1 = (bf16[2,256]{1,0:T(2,128)(2,1)S(1)}, bf16[2,256]{1,0:T(2,128)(2,1)}, u32[]{:S(2)}) copy-start(bf16[2,256]{1,0:T(2,128)(2,1)} %probe_ref.1) | copy-start | bytes 3076
  16.8 6.5 %collective-permute-start = (f32[64,512]{1,0:T(8,128)}, f32[64,512]{1,0:T(8,128)S(1)}, u32[]{:S(2)}, u32[]{:S(2)}) collective-permute-start(f32[64,512]{1,0:T(8,128)} %get-tuple-element.9), channel_id=1, source_target_pairs={{0,8},{8,0},{16,24},{24,16},{32,40},{40,32},{48,56},{56,48},{64,72... | collective-permute-start | bytes 393224 | tf_op jit(solution)/shard_map/ppermute | solution.py:424
  23.4 0.9 %copy-start = (f32[64,512]{1,0:T(8,128)S(1)}, f32[64,512]{1,0:T(8,128)}, u32[]{:S(2)}) copy-start(f32[64,512]{1,0:T(8,128)} %get-tuple-element.8.own_ref) | copy-start | bytes 393220
  24.5 7.6 %collective-permute-start.1 = (f32[64,256]{1,0:T(8,128)S(1)}, f32[64,256]{1,0:T(8,128)S(1)}, u32[]{:S(2)}, u32[]{:S(2)}) collective-permute-start(f32[64,256]{1,0:T(8,128)S(1)} %get-tuple-element.11), channel_id=1, source_target_pairs={{0,16},{8,24},{16,0},{24,8},{32,48},{40,56},{48,32},{56,40},{64,80... | collective-permute-start | bytes 196616 | tf_op jit(solution)/shard_map/ppermute | solution.py:424
  32.4 12.7 %collective-permute-start.2 = (f32[64,128]{1,0:T(8,128)S(1)}, f32[64,128]{1,0:T(8,128)S(1)}, u32[]{:S(2)}, u32[]{:S(2)}) collective-permute-start(f32[64,128]{1,0:T(8,128)S(1)} %get-tuple-element.13), channel_id=1, source_target_pairs={{0,32},{8,40},{16,48},{24,56},{32,0},{40,8},{48,16},{56,24},{64,96... | collective-permute-start | bytes 98312 | tf_op jit(solution)/shard_map/ppermute | solution.py:424

commit v5 on v4

--- a/solution.py
+++ b/solution.py
@@ -63,17 +63,6 @@
     )
 
 
-def left_after(x):
-    size = x.shape[1]
-    place = iota(x.shape, 1)
-    x = jnp.where(place < size - 1, lanes_turned(x, -1), 0.0)
-    step = 1
-    while step < size:
-        x = x + jnp.where(place < size - step, lanes_turned(x, -step), 0.0)
-        step *= 2
-    return x
-
-
 def diagonal_blocks(x):
     block = iota((BASE, x.shape[1]), 1) % HEAD // BASE
     blocks = x[:BASE]
@@ -90,7 +79,7 @@
 
 
 def local_kernel(
-    heads, place_ref, speed_ref, x_ref, wk_ref, wv_ref, wb_ref, wf_ref, extra_ref, kept_ref, sent_ref,
+    heads, place_ref, turn_ref, speed_ref, x_ref, wk_ref, wv_ref, wb_ref, wf_ref, extra_ref, kept_ref, sent_ref,
     kv_acc, small_acc, wide_ref, turned_ref, key_ref, lower_ref, inverse_ref, inner_ref, map_ref,
     blocks_ref, factor_ref
 ):
@@ -127,12 +116,22 @@
         rate = jnp.exp(speed)
         soft = jnp.maximum(decay_pre, 0.0) + jnp.log1p(jnp.exp(-jnp.abs(decay_pre)))
         beta = 1.0 / (1.0 + jnp.exp(-beta_pre))
+        gammas = [
+            dot(twice, extra_ref[s]) - rate * soft[:, s * length : (s + 1) * length] for s in range(seqs)
+        ]
+        behind_it = jnp.where(iota((length, length), 0) > iota((length, length), 1), 1.0, 0.0).astype(BF16)
+        pieces = []
+        for gamma in gammas:
+            for _ in range(3):
+                pieces.append(gamma.astype(BF16).astype(F32))
+                gamma = gamma - pieces[-1]
+        sums = dot(jnp.concatenate(pieces, axis=0).astype(BF16), behind_it)
         decays, kept = [], []
         for s in range(seqs):
-            gamma = dot(twice, extra_ref[s]) - rate * soft[:, s * length : (s + 1) * length]
-            behind = left_after(gamma)
+            own = sums[3 * half * s : 3 * half * (s + 1)]
+            behind = own[:half] + own[half : 2 * half] + own[2 * half :]
             decays.append(jnp.exp(behind))
-            kept.append(jnp.exp(gamma[:, :1] + behind[:, :1]))
+            kept.append(jnp.exp(gammas[s][:, :1] + behind[:, :1]))
         stack = jnp.concatenate([p.astype(F32) for p in split(jnp.concatenate(decays, axis=1))], axis=0)
         pick = iota((2 * half, width), 0) % half == iota((2 * half, width), 1) // HEAD
         wide_ref[...] = dot(stack.T.astype(BF16), jnp.where(pick, 1.0, 0.0).astype(BF16))
@@ -251,7 +250,7 @@
                 tiles.append(removal + jnp.where(row[:, part] == column[:, part], 1.0 - keep[:, part], 0.0))
                 tiles.append(map_ref[here, 2 * f + 128 : 2 * f + 256])
             maps.append(jnp.concatenate(tiles, axis=1))
-        shared_out(place_ref[1] % 2, maps, kept_ref, sent_ref)
+        shared_out(turn_ref[0] % 2, maps, kept_ref, sent_ref)
 
 
 def shared_out(bit, halves, kept_ref, sent_ref):
@@ -375,13 +374,14 @@
     steps = 4
     deep = depth // steps
     turn = lax.axis_index("sp").astype(jnp.int32).reshape(1)
-    place = jnp.concatenate([lax.axis_index("tp").astype(jnp.int32).reshape(1), turn])
+    place = lax.axis_index("tp").astype(jnp.int32).reshape(1)
     share = (HEAD, 2 * width)
     kept, sent = pl.pallas_call(
         functools.partial(local_kernel, heads),
         grid=(steps,),
         out_shape=(jax.ShapeDtypeStruct(share, F32),) * 2,
         in_specs=[
+            pl.BlockSpec(memory_space=pltpu.SMEM),
             pl.BlockSpec(memory_space=pltpu.SMEM),
             pl.BlockSpec(memory_space=pltpu.SMEM),
             pl.BlockSpec((seqs, length, deep), lambda i: (0, 0, i)),
@@ -409,6 +409,7 @@
         name="local_maps",
     )(
         place,
+        turn,
         logged_fading_speed,
         layer_feed,
         address_mapping,

time: 78.8 us -> 77.8 us (0.987)
  no operation moved by 1% of the time
where the time goes in v5:
time: 77.8 us; the launch traced here: 77.6 us
  blocking collectives  32.2 us (41%)
  starting transfers between devices  18.6 us (24%)
  Pallas kernels  17 us (22%)
  waiting for transfers between devices  8.19 us (11%)
  local copies, waits for them, and re-layouts  0.91 us (1%)
    all_to_all x1, blocking collectives, body(): mine = lax.all_to_all(shares, 'sp', 0, 0, tiled=True)  32.2 us
    ppermute x3, starting transfers between devices, swapped(): return lax.ppermute(x, 'sp', [(i, i ^ distance) for i in range(ways)])  18.6 us
    pallas_call x1, Pallas kernels, body(): pl.pallas_call(functools.partial(local_kernel, heads), grid=(steps,), out...  15.2 us
    ppermute x3, waiting for transfers between devices, swapped(): return lax.ppermute(x, 'sp', [(i, i ^ distance) for i in range(ways)])  8.19 us
  transfers between devices with their start and end apart: 3, of which 3 were waited for; matrix products, arithmetic and copies ran while one was open for 0% of the time, Pallas kernels for 0%

profile of v5, /device:TPU:46, one launch (start us, length us, event | category | flops | bytes accessed | tf_op | source)
XLA Modules:
  0.0 77.6 jit_solution(15877815679028685685)
XLA Ops:
  0.6 0.0 copy-start.1
  0.6 15.2 %local_maps.1 = (f32[64,512]{1,0:T(8,128)}, f32[64,512]{1,0:T(8,128)}) custom-call(s32[1]{0:T(128)} %bitcast.1.place_ref, s32[1]{0:T(128)} %bitcast.turn_ref.place_ref, f32[4]{0:T(128)} %speed_ref.1, bf16[2,512,4096]{2,1,0:T(8,128)(2,1)} %x_ref.1, bf16[4096,256]{1,0:T(8,128)(2,1)} %wk_ref.1, bf16[4096,256]{1,0:T(8,128)(2,1)} %wv_ref.1, ...), custom_call_target="tpu_custom_call" | custom-call | tf_op jit(solution)/shard_map/local_maps/pallas_call | solution.py:379
  15.8 2.8 %collective-permute-start = (f32[64,512]{1,0:T(8,128)}, f32[64,512]{1,0:T(8,128)S(1)}, u32[]{:S(2)}, u32[]{:S(2)}) collective-permute-start(f32[64,512]{1,0:T(8,128)} %get-tuple-element.9), channel_id=1, source_target_pairs={{0,8},{8,0},{16,24},{24,16},{32,40},{40,32},{48,56},{56,48},{64,72... | collective-permute-start | bytes 393224 | tf_op jit(solution)/shard_map/ppermute | solution.py:425
  18.6 3.8 %collective-permute-done.other_ref = f32[64,512]{1,0:T(8,128)S(1)} collective-permute-done((f32[64,512]{1,0:T(8,128)}, f32[64,512]{1,0:T(8,128)S(1)}, u32[]{:S(2)}, u32[]{:S(2)}) %collective-permute-start) | collective-permute-done | bytes 131104 | tf_op jit(solution)/shard_map/ppermute | solution.py:425
  22.4 0.0 copy-start
  22.4 0.9 %copy-done = f32[64,512]{1,0:T(8,128)S(1)} copy-done((f32[64,512]{1,0:T(8,128)S(1)}, f32[64,512]{1,0:T(8,128)}, u32[]{:S(2)}) %copy-start) | copy-done | bytes 131096
  23.3 0.2 first.1
  23.5 5.1 %collective-permute-start.1 = (f32[64,256]{1,0:T(8,128)S(1)}, f32[64,256]{1,0:T(8,128)S(1)}, u32[]{:S(2)}, u32[]{:S(2)}) collective-permute-start(f32[64,256]{1,0:T(8,128)S(1)} %get-tuple-element.11), channel_id=1, source_target_pairs={{0,16},{8,24},{16,0},{24,8},{32,48},{40,56},{48,32},{56,40},{64,80... | collective-permute-start | bytes 196616 | tf_op jit(solution)/shard_map/ppermute | solution.py:425
  28.6 2.5 %collective-permute-done.1.other_ref = f32[64,256]{1,0:T(8,128)S(1)} collective-permute-done((f32[64,256]{1,0:T(8,128)S(1)}, f32[64,256]{1,0:T(8,128)S(1)}, u32[]{:S(2)}, u32[]{:S(2)}) %collective-permute-start.1) | collective-permute-done | bytes 65568 | tf_op jit(solution)/shard_map/ppermute | solution.py:425
  31.1 0.2 second.1
  31.4 10.7 %collective-permute-start.2 = (f32[64,128]{1,0:T(8,128)S(1)}, f32[64,128]{1,0:T(8,128)S(1)}, u32[]{:S(2)}, u32[]{:S(2)}) collective-permute-start(f32[64,128]{1,0:T(8,128)S(1)} %get-tuple-element.13), channel_id=1, source_target_pairs={{0,32},{8,40},{16,48},{24,56},{32,0},{40,8},{48,16},{56,24},{64,96... | collective-permute-start | bytes 98312 | tf_op jit(solution)/shard_map/ppermute | solution.py:425
  42.1 1.9 %collective-permute-done.2.other_ref = f32[64,128]{1,0:T(8,128)S(1)} collective-permute-done((f32[64,128]{1,0:T(8,128)S(1)}, f32[64,128]{1,0:T(8,128)S(1)}, u32[]{:S(2)}, u32[]{:S(2)}) %collective-permute-start.2) | collective-permute-done | bytes 32800 | tf_op jit(solution)/shard_map/ppermute | solution.py:425
  44.0 0.0 copy-done.1
  44.0 0.3 third.1
  44.4 32.2 %all_to_all.5.in_ref = f32[16,32,128]{2,1,0:T(8,128)S(1)} all-to-all(f32[16,32,128]{2,1,0:T(8,128)S(1)} %third.1), channel_id=1, replica_groups=mesh['grp'=2,'sp'=16,'tp'=8] {'sp'}, dimensions={0} | all-to-all | bytes 524288 | tf_op jit(solution)/shard_map/all_to_all | solution.py:442
  76.6 1.0 %results.1 = (bf16[2,4,4,64]{3,2,1,0:T(4,128)(2,1)}, bf16[2,256]{1,0:T(2,128)(2,1)}) custom-call(f32[16,32,128]{2,1,0:T(8,128)S(1)} %all_to_all.5.in_ref), custom_call_target="tpu_custom_call" | custom-call | tf_op jit(solution)/shard_map/results/pallas_call | solution.py:443
Async XLA Ops:
  0.6 43.4 %copy-start.1 = (bf16[2,256]{1,0:T(2,128)(2,1)S(1)}, bf16[2,256]{1,0:T(2,128)(2,1)}, u32[]{:S(2)}) copy-start(bf16[2,256]{1,0:T(2,128)(2,1)} %probe_ref.1) | copy-start | bytes 3076
  15.8 6.5 %collective-permute-start = (f32[64,512]{1,0:T(8,128)}, f32[64,512]{1,0:T(8,128)S(1)}, u32[]{:S(2)}, u32[]{:S(2)}) collective-permute-start(f32[64,512]{1,0:T(8,128)} %get-tuple-element.9), channel_id=1, source_target_pairs={{0,8},{8,0},{16,24},{24,16},{32,40},{40,32},{48,56},{56,48},{64,72... | collective-permute-start | bytes 393224 | tf_op jit(solution)/shard_map/ppermute | solution.py:425
  22.4 0.9 %copy-start = (f32[64,512]{1,0:T(8,128)S(1)}, f32[64,512]{1,0:T(8,128)}, u32[]{:S(2)}) copy-start(f32[64,512]{1,0:T(8,128)} %get-tuple-element.8.own_ref) | copy-start | bytes 393220
  23.5 7.6 %collective-permute-start.1 = (f32[64,256]{1,0:T(8,128)S(1)}, f32[64,256]{1,0:T(8,128)S(1)}, u32[]{:S(2)}, u32[]{:S(2)}) collective-permute-start(f32[64,256]{1,0:T(8,128)S(1)} %get-tuple-element.11), channel_id=1, source_target_pairs={{0,16},{8,24},{16,0},{24,8},{32,48},{40,56},{48,32},{56,40},{64,80... | collective-permute-start | bytes 196616 | tf_op jit(solution)/shard_map/ppermute | solution.py:425
  31.4 12.7 %collective-permute-start.2 = (f32[64,128]{1,0:T(8,128)S(1)}, f32[64,128]{1,0:T(8,128)S(1)}, u32[]{:S(2)}, u32[]{:S(2)}) collective-permute-start(f32[64,128]{1,0:T(8,128)S(1)} %get-tuple-element.13), channel_id=1, source_target_pairs={{0,32},{8,40},{16,48},{24,56},{32,0},{40,8},{48,16},{56,24},{64,96... | collective-permute-start | bytes 98312 | tf_op jit(solution)/shard_map/ppermute | solution.py:425

commit v6 on v5

--- a/solution.py
+++ b/solution.py
@@ -379,7 +379,7 @@
     kept, sent = pl.pallas_call(
         functools.partial(local_kernel, heads),
         grid=(steps,),
-        out_shape=(jax.ShapeDtypeStruct(share, F32),) * 2,
+        out_shape=(pltpu.VMEM(share, F32),) * 2,
         in_specs=[
             pl.BlockSpec(memory_space=pltpu.SMEM),
             pl.BlockSpec(memory_space=pltpu.SMEM),

time: 77.8 us -> 76.1 us (0.978)
  local copies, waits for them, and re-layouts: 0.91 us -> 0.01 us
    unnamed x4 -> x2, local copies, waits for them, and re-layouts: 0.91 us -> 0.01 us
where the time goes in v6:
time: 76.1 us; the launch traced here: 76 us
  blocking collectives  32.2 us (42%)
  starting transfers between devices  18.8 us (25%)
  Pallas kernels  16.3 us (21%)
  waiting for transfers between devices  8.02 us (11%)
    all_to_all x1, blocking collectives, body(): mine = lax.all_to_all(shares, 'sp', 0, 0, tiled=True)  32.2 us
    ppermute x3, starting transfers between devices, swapped(): return lax.ppermute(x, 'sp', [(i, i ^ distance) for i in range(ways)])  18.8 us
    pallas_call x1, Pallas kernels, body(): pl.pallas_call(functools.partial(local_kernel, heads), grid=(steps,), out...  14.5 us
    ppermute x3, waiting for transfers between devices, swapped(): return lax.ppermute(x, 'sp', [(i, i ^ distance) for i in range(ways)])  8.02 us
  transfers between devices with their start and end apart: 3, of which 3 were waited for; matrix products, arithmetic and copies ran while one was open for 0% of the time, Pallas kernels for 0%

profile of v6, /device:TPU:46, one launch (start us, length us, event | category | flops | bytes accessed | tf_op | source)
XLA Modules:
  0.0 76.0 jit_solution(14971785570565722665)
XLA Ops:
  0.6 0.0 copy-start
  0.6 14.5 %local_maps.1 = (f32[64,512]{1,0:T(8,128)S(1)}, f32[64,512]{1,0:T(8,128)S(1)}) custom-call(s32[1]{0:T(128)} %bitcast.1.place_ref, s32[1]{0:T(128)} %bitcast.turn_ref.place_ref, f32[4]{0:T(128)} %speed_ref.1, bf16[2,512,4096]{2,1,0:T(8,128)(2,1)} %x_ref.1, bf16[4096,256]{1,0:T(8,128)(2,1)} %wk_ref.1, bf16[4096,256]{1,0:T(8,128)(2,1)} %wv_ref.1, ...), custom_call_target="tpu_custom_call" | custom-call | tf_op jit(solution)/shard_map/local_maps/pallas_call | solution.py:379
  15.1 2.9 %collective-permute-start = (f32[64,512]{1,0:T(8,128)S(1)}, f32[64,512]{1,0:T(8,128)S(1)}, u32[]{:S(2)}, u32[]{:S(2)}) collective-permute-start(f32[64,512]{1,0:T(8,128)S(1)} %get-tuple-element.9), channel_id=1, source_target_pairs={{0,8},{8,0},{16,24},{24,16},{32,40},{40,32},{48,56},{56,48},{64,72... | collective-permute-start | bytes 393224 | tf_op jit(solution)/shard_map/ppermute | solution.py:425
  18.0 3.6 %collective-permute-done.other_ref = f32[64,512]{1,0:T(8,128)S(1)} collective-permute-done((f32[64,512]{1,0:T(8,128)S(1)}, f32[64,512]{1,0:T(8,128)S(1)}, u32[]{:S(2)}, u32[]{:S(2)}) %collective-permute-start) | collective-permute-done | bytes 131104 | tf_op jit(solution)/shard_map/ppermute | solution.py:425
  21.6 0.2 first.1
  21.8 5.1 %collective-permute-start.1 = (f32[64,256]{1,0:T(8,128)S(1)}, f32[64,256]{1,0:T(8,128)S(1)}, u32[]{:S(2)}, u32[]{:S(2)}) collective-permute-start(f32[64,256]{1,0:T(8,128)S(1)} %get-tuple-element.11), channel_id=1, source_target_pairs={{0,16},{8,24},{16,0},{24,8},{32,48},{40,56},{48,32},{56,40},{64,80... | collective-permute-start | bytes 196616 | tf_op jit(solution)/shard_map/ppermute | solution.py:425
  26.9 2.5 %collective-permute-done.1.other_ref = f32[64,256]{1,0:T(8,128)S(1)} collective-permute-done((f32[64,256]{1,0:T(8,128)S(1)}, f32[64,256]{1,0:T(8,128)S(1)}, u32[]{:S(2)}, u32[]{:S(2)}) %collective-permute-start.1) | collective-permute-done | bytes 65568 | tf_op jit(solution)/shard_map/ppermute | solution.py:425
  29.4 0.2 second.1
  29.7 10.8 %collective-permute-start.2 = (f32[64,128]{1,0:T(8,128)S(1)}, f32[64,128]{1,0:T(8,128)S(1)}, u32[]{:S(2)}, u32[]{:S(2)}) collective-permute-start(f32[64,128]{1,0:T(8,128)S(1)} %get-tuple-element.13), channel_id=1, source_target_pairs={{0,32},{8,40},{16,48},{24,56},{32,0},{40,8},{48,16},{56,24},{64,96... | collective-permute-start | bytes 98312 | tf_op jit(solution)/shard_map/ppermute | solution.py:425
  40.4 2.0 %collective-permute-done.2.other_ref = f32[64,128]{1,0:T(8,128)S(1)} collective-permute-done((f32[64,128]{1,0:T(8,128)S(1)}, f32[64,128]{1,0:T(8,128)S(1)}, u32[]{:S(2)}, u32[]{:S(2)}) %collective-permute-start.2) | collective-permute-done | bytes 32800 | tf_op jit(solution)/shard_map/ppermute | solution.py:425
  42.4 0.0 copy-done
  42.4 0.3 third.1
  42.8 32.2 %all_to_all.5.in_ref = f32[16,32,128]{2,1,0:T(8,128)S(1)} all-to-all(f32[16,32,128]{2,1,0:T(8,128)S(1)} %third.1), channel_id=1, replica_groups=mesh['grp'=2,'sp'=16,'tp'=8] {'sp'}, dimensions={0} | all-to-all | bytes 524288 | tf_op jit(solution)/shard_map/all_to_all | solution.py:442
  75.0 1.0 %results.1 = (bf16[2,4,4,64]{3,2,1,0:T(4,128)(2,1)}, bf16[2,256]{1,0:T(2,128)(2,1)}) custom-call(f32[16,32,128]{2,1,0:T(8,128)S(1)} %all_to_all.5.in_ref), custom_call_target="tpu_custom_call" | custom-call | tf_op jit(solution)/shard_map/results/pallas_call | solution.py:443
Async XLA Ops:
  0.6 41.8 %copy-start = (bf16[2,256]{1,0:T(2,128)(2,1)S(1)}, bf16[2,256]{1,0:T(2,128)(2,1)}, u32[]{:S(2)}) copy-start(bf16[2,256]{1,0:T(2,128)(2,1)} %probe_ref.1) | copy-start | bytes 3076
  15.1 6.5 %collective-permute-start = (f32[64,512]{1,0:T(8,128)S(1)}, f32[64,512]{1,0:T(8,128)S(1)}, u32[]{:S(2)}, u32[]{:S(2)}) collective-permute-start(f32[64,512]{1,0:T(8,128)S(1)} %get-tuple-element.9), channel_id=1, source_target_pairs={{0,8},{8,0},{16,24},{24,16},{32,40},{40,32},{48,56},{56,48},{64,72... | collective-permute-start | bytes 393224 | tf_op jit(solution)/shard_map/ppermute | solution.py:425
  21.8 7.6 %collective-permute-start.1 = (f32[64,256]{1,0:T(8,128)S(1)}, f32[64,256]{1,0:T(8,128)S(1)}, u32[]{:S(2)}, u32[]{:S(2)}) collective-permute-start(f32[64,256]{1,0:T(8,128)S(1)} %get-tuple-element.11), channel_id=1, source_target_pairs={{0,16},{8,24},{16,0},{24,8},{32,48},{40,56},{48,32},{56,40},{64,80... | collective-permute-start | bytes 196616 | tf_op jit(solution)/shard_map/ppermute | solution.py:425
  29.7 12.7 %collective-permute-start.2 = (f32[64,128]{1,0:T(8,128)S(1)}, f32[64,128]{1,0:T(8,128)S(1)}, u32[]{:S(2)}, u32[]{:S(2)}) collective-permute-start(f32[64,128]{1,0:T(8,128)S(1)} %get-tuple-element.13), channel_id=1, source_target_pairs={{0,32},{8,40},{16,48},{24,56},{32,0},{40,8},{48,16},{56,24},{64,96... | collective-permute-start | bytes 98312 | tf_op jit(solution)/shard_map/ppermute | solution.py:425
